TPU v7x, 32 devices: a whole 2x2x4 slice. The times are simulated.
32 devices in a mesh: sp: 4 (over z), dp: 8 (over y, x, core).
Axes of the slice: x: 2, y: 2, z: 4, core: 2. Of those that a mesh axis runs over, the one named last changes fastest.
Arguments:
- tokens: bfloat16 [8, 768, 2048], P('dp', 'sp'), may hold values from -36 to 36
- query_weight: bfloat16 [2048, 2048], P('dp'), may hold values from -0.125 to 0.125
- key_weight: bfloat16 [2048, 512], P('dp'), may hold values from -0.125 to 0.125
- value_weight: bfloat16 [2048, 512], P('dp'), may hold values from -0.125 to 0.125
- forget_weight: bfloat16 [2048, 16], replicated, may hold values from -0.125 to 0.125
- forget_bias: float32 [16], replicated, may hold values from 3.4 to 9
Outputs:
- mixed: bfloat16 [8, 768, 2048], P('dp', 'sp')
All inputs are finite; a program needn't handle non-finite values.
Results may differ from a plain program's by a relative error of at most 0.012.
Values may be sent and summed in bfloat16 or wider, within the bound.
No kernel may reach another device: no remote copies, remote signals or barrier semaphores. Data moves between devices by JAX's collectives and lax.ppermute only.
A program may use at most 64 MiB of HBM per device.

v0:
```python
import jax
import jax.numpy as jnp
from jax import lax
from jax.sharding import PartitionSpec as P


def pick_block(length):
    for candidate in (512, 384, 256, 128):
        if length % candidate == 0:
            return candidate
    return length


def on_device(tokens, query_weight, key_weight, value_weight, forget_weight, forget_bias):
    token_rows = tokens[0]
    row_count = token_rows.shape[0]
    sp_count = lax.axis_size("sp")
    head_count = forget_weight.shape[1]
    query_width = query_weight.shape[1]
    key_width = key_weight.shape[1]
    head_dim = query_width // head_count
    key_heads = key_width // head_dim
    pieces = (
        lax.all_gather(query_weight, "dp", axis=0, tiled=True),
        lax.all_gather(key_weight, "dp", axis=0, tiled=True),
        lax.all_gather(value_weight, "dp", axis=0, tiled=True),
    )
    query_rows, key_rows, value_rows = tuple(
        (
            jnp.dot(token_rows, weight_piece, preferred_element_type=jnp.float32)
            for weight_piece in pieces
        )
    )
    query_rows = query_rows.astype(jnp.bfloat16)
    key_rows = key_rows.astype(jnp.bfloat16)
    value_rows = value_rows.astype(jnp.bfloat16)
    gate_input = (
        jnp.dot(token_rows, forget_weight, preferred_element_type=jnp.float32)
        + forget_bias[None, :]
    )
    log_gate = jax.nn.log_sigmoid(gate_input).astype(jnp.bfloat16)
    repeats = max(1, sp_count // key_heads)
    if repeats > 1:
        key_rows = jnp.repeat(key_rows.reshape(row_count, key_heads, head_dim), repeats, axis=1)
        key_rows = key_rows.reshape(row_count, key_heads * repeats * head_dim)
        value_rows = jnp.repeat(value_rows.reshape(row_count, key_heads, head_dim), repeats, axis=1)
        value_rows = value_rows.reshape(row_count, key_heads * repeats * head_dim)
    head_query, head_keys, head_values, head_gates = (
        lax.all_to_all(query_rows, "sp", split_axis=1, concat_axis=0, tiled=True),
        lax.all_to_all(key_rows, "sp", split_axis=1, concat_axis=0, tiled=True),
        lax.all_to_all(value_rows, "sp", split_axis=1, concat_axis=0, tiled=True),
        lax.all_to_all(log_gate, "sp", split_axis=1, concat_axis=0, tiled=True),
    )
    seq_length = head_query.shape[0]
    local_heads = head_count // sp_count
    local_keys = head_keys.shape[1] // head_dim
    group_share = local_heads // local_keys
    decay_sum = jnp.cumsum(head_gates.astype(jnp.float32), axis=0)
    decay_grid = decay_sum.T.reshape(local_keys, group_share, seq_length)
    grouped = head_query.reshape(seq_length, local_keys, group_share, head_dim)
    key_grid = head_keys.reshape(seq_length, local_keys, head_dim)
    value_grid = head_values.reshape(seq_length, local_keys, head_dim)
    block_size = pick_block(seq_length)
    block_count = seq_length // block_size
    score_scale = head_dim ** (-0.5)
    offsets = jnp.arange(block_size, dtype=jnp.int32)

    def query_block(block_index):
        first_row = block_index * block_size
        query_part = lax.dynamic_slice_in_dim(grouped, first_row, block_size, 0)
        query_decay = lax.dynamic_slice_in_dim(decay_grid, first_row, block_size, 2)

        def fill_scores(key_block, buffer):
            key_first = key_block * block_size
            key_part = lax.dynamic_slice_in_dim(key_grid, key_first, block_size, 0)
            key_decay = lax.dynamic_slice_in_dim(decay_grid, key_first, block_size, 2)
            raw_scores = jnp.einsum(
                "qkgd,skd->kgqs", query_part, key_part, preferred_element_type=jnp.float32
            )
            biased = raw_scores * score_scale + query_decay[..., :, None] - key_decay[..., None, :]
            allowed = (key_first + offsets)[None, :] <= (first_row + offsets)[:, None]
            masked = jnp.where(allowed, biased, -jnp.inf)
            return lax.dynamic_update_index_in_dim(buffer, masked, key_block, 0)

        score_buffer = lax.fori_loop(
            0,
            block_index + 1,
            fill_scores,
            jnp.full(
                (block_count, local_keys, group_share, block_size, block_size),
                -jnp.inf,
                jnp.float32,
            ),
        )
        row_max = jnp.max(jnp.max(score_buffer, axis=-1), axis=0)
        row_sum = jnp.sum(
            jnp.sum(jnp.exp(score_buffer - row_max[None, ..., None]), axis=-1), axis=0
        )

        def weighted(key_block, accumulated):
            block_scores = lax.dynamic_index_in_dim(score_buffer, key_block, 0, keepdims=False)
            weights = (jnp.exp(block_scores - row_max[..., None]) / row_sum[..., None]).astype(
                jnp.bfloat16
            )
            value_part = lax.dynamic_slice_in_dim(value_grid, key_block * block_size, block_size, 0)
            return accumulated + jnp.einsum(
                "kgqs,skd->qkgd", weights, value_part, preferred_element_type=jnp.float32
            )

        mixed_block = lax.fori_loop(
            0,
            block_index + 1,
            weighted,
            jnp.zeros((block_size, local_keys, group_share, head_dim), jnp.float32),
        )
        return mixed_block.astype(jnp.bfloat16).reshape(block_size, local_heads * head_dim)

    head_mixed = lax.map(query_block, jnp.arange(block_count, dtype=jnp.int32))
    head_mixed = head_mixed.reshape(seq_length, local_heads * head_dim)
    mixed = lax.all_to_all(head_mixed, "sp", split_axis=0, concat_axis=1, tiled=True)
    return mixed[None]


def solution(mesh):
    placed = (P("dp", "sp", None), P("dp", None), P("dp", None), P("dp", None), P(), P())
    return jax.shard_map(
        on_device, mesh=mesh, in_specs=placed, out_specs=P("dp", "sp", None), check_vma=False
    )
```

profile of v0, /device:TPU:0, one launch (start us, length us, event | category | flops | bytes accessed | tf_op | source)
XLA Modules:
  0.0 229.2 jit_solution(9578474785940461810)
XLA Ops:
  6.5 0.7 all-gather.8.cloned.1.call-update
  7.3 0.7 all-gather.4.cloned.1.call-update
  8.1 0.7 all-gather.6.cloned.1.call-update
  8.8 1.2 fusion.23
  9.9 0.6 all_to_all.61
  10.5 6.3 %all-to-all-start.1 = ((bf16[192,4,4]{0,2,1:T(4,128)(2,1)}), bf16[192,4,4]{0,2,1:T(4,128)(2,1)S(1)}, u32[]{:S(2)}, u32[]{:S(2)}) async-start(bf16[192,4,4]{0,2,1:T(4,128)(2,1)} %all_to_all.61), calls=%async_computation.1 | async-start | bytes 16384 | tf_op jit(solution)/shard_map/all_to_all | solution.py:52
  16.9 22.9 %all-gather.8.cloned.1.call-done = bf16[2048,512]{1,0:T(8,128)(2,1)} async-done(((bf16[256,512]{1,0:T(8,128)(2,1)}), bf16[2048,512]{1,0:T(8,128)(2,1)}) %all-gather.8.cloned.1.call-update) | async-done | bytes 2097168 | tf_op jit(solution)/shard_map/all_gather | solution.py:26
  39.8 2.2 fusion.16
  41.9 0.7 copy.47
  42.6 4.6 %all-to-all-start.3 = ((bf16[192,4,128]{2,0,1:T(8,128)(2,1)}), bf16[192,4,128]{2,0,1:T(8,128)(2,1)S(1)}, u32[]{:S(2)}, u32[]{:S(2)}) async-start(bf16[192,4,128]{2,0,1:T(8,128)(2,1)} %bitcast.89), calls=%async_computation.3 | async-start | bytes 393216 | tf_op jit(solution)/shard_map/all_to_all | solution.py:51
  47.2 48.7 %all-gather.4.cloned.1.call-done = bf16[2048,2048]{1,0:T(8,128)(2,1)} async-done(((bf16[256,2048]{1,0:T(8,128)(2,1)}), bf16[2048,2048]{1,0:T(8,128)(2,1)}) %all-gather.4.cloned.1.call-update) | async-done | bytes 8388624 | tf_op jit(solution)/shard_map/all_gather | solution.py:24
  95.9 5.2 %convolution_convert_fusion = bf16[192,2048]{1,0:T(8,128)(2,1)S(1)} fusion(bf16[2048,2048]{1,0:T(8,128)(2,1)} %all-gather.4.cloned.1.call-done, bf16[1,192,2048]{2,1,0:T(8,128)(2,1)S(1)} %copy-done), kind=kOutput, calls=%fused_computation.26 | convolution fusion | flops 1611005952 | bytes 9961472 | tf_op jit(solution)/shard_map/dot_general | solution.py:30
  101.1 0.9 copy.46
  102.1 4.6 %all-to-all-start = ((bf16[192,4,512]{2,0,1:T(8,128)(2,1)}), bf16[192,4,512]{2,0,1:T(8,128)(2,1)S(1)}, u32[]{:S(2)}, u32[]{:S(2)}) async-start(bf16[192,4,512]{2,0,1:T(8,128)(2,1)} %bitcast.88), calls=%async_computation | async-start | bytes 1572864 | tf_op jit(solution)/shard_map/all_to_all | solution.py:49
  106.8 1.1 reduce-window.6
  107.9 17.7 %all-gather.6.cloned.1.call-done = bf16[2048,512]{1,0:T(8,128)(2,1)} async-done(((bf16[256,512]{1,0:T(8,128)(2,1)}), bf16[2048,512]{1,0:T(8,128)(2,1)}) %all-gather.6.cloned.1.call-update) | async-done | bytes 2097168 | tf_op jit(solution)/shard_map/all_gather | solution.py:25
  125.6 2.2 fusion.15
  127.8 0.7 copy.48
  128.5 4.6 %all-to-all-start.2 = ((bf16[192,4,128]{2,0,1:T(8,128)(2,1)}), bf16[192,4,128]{2,0,1:T(8,128)(2,1)S(1)}, u32[]{:S(2)}, u32[]{:S(2)}) async-start(bf16[192,4,128]{2,0,1:T(8,128)(2,1)} %bitcast.90), calls=%async_computation.2 | async-start | bytes 393216 | tf_op jit(solution)/shard_map/all_to_all | solution.py:50
  133.1 0.2 slice_reduce_fusion
  133.3 0.2 reduce-window.9
  133.6 0.8 copy.33
  134.4 1.1 reshape.109
  135.4 5.6 %all-to-all-done.2 = bf16[192,4,128]{2,0,1:T(8,128)(2,1)S(1)} async-done(((bf16[192,4,128]{2,0,1:T(8,128)(2,1)}), bf16[192,4,128]{2,0,1:T(8,128)(2,1)S(1)}, u32[]{:S(2)}, u32[]{:S(2)}) %all-to-all-start.2) | async-done | bytes 196640 | tf_op jit(solution)/shard_map/all_to_all | solution.py:50
  141.0 57.3 %while.39 = (s32[]{:T(128)}, bf16[2,384,512]{2,1,0:T(8,128)(2,1)}, s32[2]{0:T(128)S(1)}, bf16[768,1,4,128]{3,2,0,1:T(4,128)(2,1)}, f32[1,4,768]{2,1,0:T(4,128)S(...) while((s32[]{:T(128)}, bf16[2,384,512]{2,1,0:T(8,128)(2,1)}, ...), condition=%wide.region_9.10_spmd.clone.clone, body=%wide.region_2.0_spmd.clone.clone.sunk | while | flops 310195968 | bytes 35959236 | solution.py:118
  141.0 0.6 dynamic_slice.52
  142.2 1.1 constant_dynamic-slice_fusion.6
  144.0 2.5 %broadcast.53 = f32[2,1,4,384,384]{3,4,2,1,0:T(8,128)} broadcast(f32[]{:T(128)} %constant.52.clone.3..sunk), dimensions={} | broadcast | bytes 4718596 | tf_op jit(solution)/shard_map/broadcast.5
  146.5 2.2 while.40
  146.5 0.1 broadcast_compare_fusion.2
  146.7 2.0 fusion.38
  148.7 2.6 %reduce_max.20 = f32[4,384]{1,0:T(4,128)S(1)} reduce(f32[2,1,4,384,384]{3,4,2,1,0:T(8,128)} %get-tuple-element.530, f32[]{:T(128)} %constant.52.clone.3..sunk), dimensions={0,1,4}, to_apply=%region_5.5 | reduce | flops 1178112 | bytes 4724740 | tf_op jit(solution)/shard_map/while/body/eval_jaxpr/reduce_max | solution.py:95
  151.3 3.0 %exponential_reduce_fusion.2 = f32[4,384]{1,0:T(4,128)S(1)} fusion(f32[2,1,4,384,384]{3,4,2,1,0:T(8,128)} %get-tuple-element.530, f32[4,384]{1,0:T(4,128)S(1)} %reduce_max.20), kind=kLoop, calls=%fused_computation.22.clone.1 | loop fusion | flops 2357760 | bytes 4730880 | tf_op jit(solution)/shard_map/while/body/eval_jaxpr/reduce_sum | solution.py:96
  154.2 1.0 broadcast.52
  155.3 7.4 %while.41 = (s32[]{:T(128)}, f32[384,1,4,128]{0,3,2,1:T(8,128)}, s32[]{:T(128)}, bf16[768,1,128]{0,2,1:T(8,128)(2,1)}, f32[2,1,4,384,384]{3,4,2,1,0:T(8,128)}, /...) while((s32[]{:T(128)}, f32[384,1,4,128]{0,3,2,1:T(8,128)}, ...), condition=%wide.region_8.8_spmd, body=%wide.region_7.7_spmd.sunk | while | flops 152961024 | bytes 13480141 | solution.py:110
  155.3 1.8 constant_dynamic-slice_fusion.8
  157.1 2.0 copy.54
  159.1 3.6 %fusion.41 = f32[384,1,4,128]{0,3,2,1:T(8,128)} fusion(f32[384,1,4,128]{0,3,2,1:T(8,128)} %get-tuple-element.539, f32[1,1,4,384,384]{4,3,2,1,0:T(8,128)} %copy.54, f32[4,384]{1,0:T(4,128)S(1)} %bitcast.135, f32[4,384]{1,0:T(4,128)S(1)} %bitcast.131, bf16[768,1,128]{0,2,1:T(8,128)(2,1)} %get-tuple-element.553, s32[]{:T(128)S(6)} %select_n.55), kind=kOutput, calls=%fused_computation.3.clone.1 | convolution fusion | flops 152961024 | bytes 4042756 | tf_op jit(solution)/shard_map/while/body/eval_jaxpr/while/body/kgqs,skd->qkgd/dot_general | solution.py:106
  162.7 1.2 convert_element_type.53
  163.9 0.2 copy.53
  164.1 0.8 constant_dynamic-update-slice_fusion.2
  164.9 0.6 dynamic_slice.52
  166.0 1.1 constant_dynamic-slice_fusion.6
  167.8 2.5 %broadcast.53 = f32[2,1,4,384,384]{3,4,2,1,0:T(8,128)} broadcast(f32[]{:T(128)} %constant.52.clone.3..sunk), dimensions={} | broadcast | bytes 4718596 | tf_op jit(solution)/shard_map/broadcast.5
  170.3 4.4 %while.40 = (s32[]{:T(128)}, f32[2,1,4,384,384]{3,4,2,1,0:T(8,128)}, s32[]{:T(128)}, s32[384]{0:T(512)S(1)}, s32[]{:T(128)}, /*index=5*/bf16[768,1,128]{2,0,1:T(...) while((s32[]{:T(128)}, ...), condition=%wide.region_4.4_spmd.clone, body=%wide.region_3.3_spmd.clone.sunk | while | flops 153502464 | bytes 3178217 | solution.py:85
  170.5 2.0 fusion.38
  172.5 0.1 broadcast_compare_fusion.2
  172.7 2.0 fusion.38
  174.7 2.6 %reduce_max.20 = f32[4,384]{1,0:T(4,128)S(1)} reduce(f32[2,1,4,384,384]{3,4,2,1,0:T(8,128)} %get-tuple-element.530, f32[]{:T(128)} %constant.52.clone.3..sunk), dimensions={0,1,4}, to_apply=%region_5.5 | reduce | flops 1178112 | bytes 4724740 | tf_op jit(solution)/shard_map/while/body/eval_jaxpr/reduce_max | solution.py:95
  177.3 3.0 %exponential_reduce_fusion.2 = f32[4,384]{1,0:T(4,128)S(1)} fusion(f32[2,1,4,384,384]{3,4,2,1,0:T(8,128)} %get-tuple-element.530, f32[4,384]{1,0:T(4,128)S(1)} %reduce_max.20), kind=kLoop, calls=%fused_computation.22.clone.1 | loop fusion | flops 2357760 | bytes 4730880 | tf_op jit(solution)/shard_map/while/body/eval_jaxpr/reduce_sum | solution.py:96
  180.3 1.0 broadcast.52
  181.3 14.9 %while.41 = (s32[]{:T(128)}, f32[384,1,4,128]{0,3,2,1:T(8,128)}, s32[]{:T(128)}, bf16[768,1,128]{0,2,1:T(8,128)(2,1)}, f32[2,1,4,384,384]{3,4,2,1,0:T(8,128)}, /...) while((s32[]{:T(128)}, f32[384,1,4,128]{0,3,2,1:T(8,128)}, ...), condition=%wide.region_8.8_spmd, body=%wide.region_7.7_spmd.sunk | while | flops 152961024 | bytes 13480141 | solution.py:110
  181.3 1.8 constant_dynamic-slice_fusion.8
  183.1 2.0 copy.54
  185.1 3.6 %fusion.41 = f32[384,1,4,128]{0,3,2,1:T(8,128)} fusion(f32[384,1,4,128]{0,3,2,1:T(8,128)} %get-tuple-element.539, f32[1,1,4,384,384]{4,3,2,1,0:T(8,128)} %copy.54, f32[4,384]{1,0:T(4,128)S(1)} %bitcast.135, f32[4,384]{1,0:T(4,128)S(1)} %bitcast.131, bf16[768,1,128]{0,2,1:T(8,128)(2,1)} %get-tuple-element.553, s32[]{:T(128)S(6)} %select_n.55), kind=kOutput, calls=%fused_computation.3.clone.1 | convolution fusion | flops 152961024 | bytes 4042756 | tf_op jit(solution)/shard_map/while/body/eval_jaxpr/while/body/kgqs,skd->qkgd/dot_general | solution.py:106
  188.7 1.8 constant_dynamic-slice_fusion.8
  190.6 2.0 copy.54
  192.6 3.6 %fusion.41 = f32[384,1,4,128]{0,3,2,1:T(8,128)} fusion(f32[384,1,4,128]{0,3,2,1:T(8,128)} %get-tuple-element.539, f32[1,1,4,384,384]{4,3,2,1,0:T(8,128)} %copy.54, f32[4,384]{1,0:T(4,128)S(1)} %bitcast.135, f32[4,384]{1,0:T(4,128)S(1)} %bitcast.131, bf16[768,1,128]{0,2,1:T(8,128)(2,1)} %get-tuple-element.553, s32[]{:T(128)S(6)} %select_n.55), kind=kOutput, calls=%fused_computation.3.clone.1 | convolution fusion | flops 152961024 | bytes 4042756 | tf_op jit(solution)/shard_map/while/body/eval_jaxpr/while/body/kgqs,skd->qkgd/dot_general | solution.py:106
  196.2 1.2 convert_element_type.53
  197.4 0.2 copy.53
  197.6 0.8 constant_dynamic-update-slice_fusion.2
  198.3 22.2 %all_to_all.77 = bf16[4,192,512]{2,1,0:T(8,128)(2,1)S(1)} all-to-all(bf16[4,192,512]{2,1,0:T(8,128)(2,1)} %bitcast.127), channel_id=1, replica_groups=mesh['sp'=4,'dp'=8] {'sp'}, dimensions={0} | all-to-all | bytes 1572864 | tf_op jit(solution)/shard_map/all_to_all | solution.py:120
  220.6 0.6 copy.35
  221.2 1.5 broadcast_in_dim.31
  (29 shorter events, 0.6 us)
Async XLA Ops:
  6.5 2.2 copy-start
  6.5 33.2 %all-gather.8.cloned.1.call-start = ((), (), s32[]{:S(2)}) async-start(), calls=%async_computation.7 | async-start | bytes 2359296 | tf_op jit(solution)/shard_map/all_gather | solution.py:26
  7.3 88.7 %all-gather.4.cloned.1.call-start = ((), (), s32[]{:S(2)}) async-start(), calls=%async_computation.5 | async-start | bytes 9437184 | tf_op jit(solution)/shard_map/all_gather | solution.py:24
  8.0 117.6 %all-gather.6.cloned.1.call-start = ((), (), s32[]{:S(2)}) async-start(), calls=%async_computation.6 | async-start | bytes 2359296 | tf_op jit(solution)/shard_map/all_gather | solution.py:25
  10.5 32.1 %all-to-all-start.1 = ((bf16[192,4,4]{0,2,1:T(4,128)(2,1)}), bf16[192,4,4]{0,2,1:T(4,128)(2,1)S(1)}, u32[]{:S(2)}, u32[]{:S(2)}) async-start(bf16[192,4,4]{0,2,1:T(4,128)(2,1)} %all_to_all.61), calls=%async_computation.1 | async-start | bytes 16384 | tf_op jit(solution)/shard_map/all_to_all | solution.py:52
  42.6 59.4 %all-to-all-start.3 = ((bf16[192,4,128]{2,0,1:T(8,128)(2,1)}), bf16[192,4,128]{2,0,1:T(8,128)(2,1)S(1)}, u32[]{:S(2)}, u32[]{:S(2)}) async-start(bf16[192,4,128]{2,0,1:T(8,128)(2,1)} %bitcast.89), calls=%async_computation.3 | async-start | bytes 393216 | tf_op jit(solution)/shard_map/all_to_all | solution.py:51
  102.1 26.5 %all-to-all-start = ((bf16[192,4,512]{2,0,1:T(8,128)(2,1)}), bf16[192,4,512]{2,0,1:T(8,128)(2,1)S(1)}, u32[]{:S(2)}, u32[]{:S(2)}) async-start(bf16[192,4,512]{2,0,1:T(8,128)(2,1)} %bitcast.88), calls=%async_computation | async-start | bytes 1572864 | tf_op jit(solution)/shard_map/all_to_all | solution.py:49
  128.5 12.5 %all-to-all-start.2 = ((bf16[192,4,128]{2,0,1:T(8,128)(2,1)}), bf16[192,4,128]{2,0,1:T(8,128)(2,1)S(1)}, u32[]{:S(2)}, u32[]{:S(2)}) async-start(bf16[192,4,128]{2,0,1:T(8,128)(2,1)} %bitcast.90), calls=%async_computation.2 | async-start | bytes 393216 | tf_op jit(solution)/shard_map/all_to_all | solution.py:50
Sparse Core Ops, SparseCore 0:
  9.2 30.4 all-gather.7
  41.6 54.2 all-gather.3
  97.8 27.7 all-gather.5
where the time goes:
time: 230 us; the launch traced here: 229 us
  waiting for transfers between devices  97 us (42%)
  local copies, waits for them, and re-layouts  31.3 us (14%)
  matrix products  27.6 us (12%)
  blocking collectives  22.2 us (10%)
  starting transfers between devices  20.2 us (9%)
  other arithmetic  15.3 us (7%)
  between operations  13.2 us (6%)
  loops' own time  2.43 us (1%)
    all_gather x1, waiting for transfers between devices, on_device(): lax.all_gather(query_weight, 'dp', axis=0, tiled=True)  48.7 us
    all_gather x1, waiting for transfers between devices, on_device(): lax.all_gather(value_weight, 'dp', axis=0, tiled=True)  22.9 us
    all_to_all x1, blocking collectives, on_device(): lax.all_to_all(head_mixed, 'sp', split_axis=0, concat_axis=1, tiled=True)  22.2 us
    all_gather x1, waiting for transfers between devices, on_device(): lax.all_gather(key_weight, 'dp', axis=0, tiled=True)  17.7 us
    dynamic_slice x6, local copies, waits for them, and re-layouts, weighted(): lax.dynamic_index_in_dim(score_buffer, key_block, 0, keepdims=False)  11.5 us
    dot_general x3, matrix products, weighted(): jnp.einsum('kgqs,skd->qkgd', weights, value_part, preferred_element_type=...  10.8 us
    dot_general x3, matrix products, on_device(): jnp.dot(token_rows, weight_piece, preferred_element_type=jnp.float32)  9.52 us
    another operation x8, local copies, waits for them, and re-layouts  7.22 us
  transfers between devices with their start and end apart: 7, of which 4 were waited for; matrix products, arithmetic and copies ran while one was open for 7% of the time, Pallas kernels for 0%

commit v1 on v0

--- a/solution.py
+++ b/solution.py
@@ -1,7 +1,282 @@
+import functools
+import math
+
 import jax
 import jax.numpy as jnp
 from jax import lax
+from jax.experimental import pallas as pl
+from jax.experimental.pallas import tpu as pltpu
 from jax.sharding import PartitionSpec as P
+
+VMEM_SPEC = pl.BlockSpec(memory_space=pltpu.VMEM)
+FAR = 1e30
+GATE_ROWS = 16
+HEAD_PAD = 8
+NT = (((1,), (1,)), ((), ()))
+
+
+def core_swap(dp_count):
+    return [(i, i ^ 1) for i in range(dp_count)]
+
+
+def first_hop(dp_count):
+    return [(i, i ^ (4 if i & 1 else 2)) for i in range(dp_count)]
+
+
+def second_hop(dp_count):
+    return [(i, i ^ (2 if i & 1 else 4)) for i in range(dp_count)]
+
+
+def chip_sources():
+    device = lax.axis_index("dp")
+    core = lax.rem(device, 2)
+    chip = lax.div(device, 2)
+    near = jnp.where(core == 0, 1, 2)
+    far = jnp.where(core == 0, 2, 1)
+    return core, [chip, chip ^ near, chip ^ far, chip ^ 3]
+
+
+def shard_columns(chip, core, depth):
+    first = pl.multiple_of((chip * 2 + core) * depth, depth)
+    second = pl.multiple_of((chip * 2 + 1 - core) * depth, depth)
+    return pl.ds(first, depth), pl.ds(second, depth)
+
+
+def chip_product(x_refs, weight_ref, chip, core):
+    depth = weight_ref.shape[0] // 2
+    total = None
+    for half, columns in enumerate(shard_columns(chip, core, depth)):
+        rows = jnp.concatenate([x_ref[:, columns] for x_ref in x_refs], axis=0)
+        term = jnp.dot(
+            rows, weight_ref[half * depth : (half + 1) * depth, :], preferred_element_type=jnp.float32
+        )
+        total = term if total is None else total + term
+    return total
+
+
+def kv_kernel(xh_ref, xo_ref, w0_ref, wa_ref, wb_ref, wab_ref, wf_ref, bias_ref, out_ref):
+    core, chips = chip_sources()
+    rows = xh_ref.shape[0]
+    total = None
+    for chip, weight_ref in zip(chips, (w0_ref, wa_ref, wb_ref, wab_ref)):
+        term = chip_product((xh_ref, xo_ref), weight_ref, chip, core)
+        total = term if total is None else total + term
+    for n, x_ref in enumerate((xh_ref, xo_ref)):
+        out_ref[n, :rows, :] = total[n * rows : (n + 1) * rows].astype(jnp.bfloat16)
+        logit = lax.dot_general(wf_ref[...], x_ref[...], NT, preferred_element_type=jnp.float32)
+        logit = logit + bias_ref[:, 0:1]
+        gate = jnp.minimum(logit, 0.0) - jnp.log1p(jnp.exp(-jnp.abs(logit)))
+        pad = out_ref.shape[2] - rows
+        wide = jnp.concatenate([gate, jnp.zeros((HEAD_PAD, pad), jnp.float32)], axis=1)
+        tall = jnp.concatenate([wide, jnp.zeros_like(wide)], axis=0)
+        out_ref[n, rows:, :] = tall.astype(jnp.bfloat16)
+
+
+def project_kv(xh, xo, weights, wf, bias):
+    rows, width = xh.shape[0], weights[0].shape[1]
+    flops = 2 * 2 * rows * xh.shape[1] * width
+    return pl.pallas_call(
+        kv_kernel,
+        out_shape=jax.ShapeDtypeStruct((2, rows + GATE_ROWS, width), jnp.bfloat16),
+        in_specs=[VMEM_SPEC] * 8,
+        out_specs=VMEM_SPEC,
+        cost_estimate=pl.CostEstimate(flops=flops, bytes_accessed=2 * xh.size * 2, transcendentals=0),
+        name="project_kv",
+    )(xh, xo, *weights, wf, bias)
+
+
+def q_kernel(xa_ref, xb_ref, xc_ref, xd_ref, w0_ref, wa_ref, wb_ref, out_ref):
+    core, chips = chip_sources()
+    rows = xa_ref.shape[0]
+    total = None
+    for chip, weight_ref in zip(chips, (w0_ref, wa_ref, wb_ref)):
+        term = chip_product((xa_ref, xb_ref, xc_ref, xd_ref), weight_ref, chip, core)
+        total = term if total is None else total + term
+    for n in range(4):
+        out_ref[n] = total[n * rows : (n + 1) * rows]
+
+
+def project_q(xs, weights):
+    rows, width = xs[0].shape[0], weights[0].shape[1]
+    flops = 2 * 4 * rows * 3 * weights[0].shape[0] * width
+    return pl.pallas_call(
+        q_kernel,
+        out_shape=jax.ShapeDtypeStruct((4, rows, width), jnp.float32),
+        in_specs=[VMEM_SPEC] * 7,
+        out_specs=VMEM_SPEC,
+        cost_estimate=pl.CostEstimate(flops=flops, bytes_accessed=4 * xs[0].size * 2, transcendentals=0),
+        name="project_q",
+    )(*xs, *weights)
+
+
+def attend_kernel(
+    partner, scale, acc_ref, xh_ref, xo_ref, w_ref, own_ref, par_ref, lown_ref, lpar_ref, outh_ref, outo_ref
+):
+    core, chips = chip_sources()
+    place = lax.axis_index("sp")
+    late = lax.rem(place, 2) == 1
+    upper = place >= 2
+    rows = xh_ref.shape[0]
+    head_dim = own_ref.shape[2] // 2
+    heads = w_ref.shape[1] // head_dim
+    log2e = math.log2(math.e)
+    above = lax.broadcasted_iota(jnp.int32, (rows, rows), 0) <= lax.broadcasted_iota(
+        jnp.int32, (rows, rows), 1
+    )
+    below = lax.broadcasted_iota(jnp.int32, (rows, rows), 0) >= lax.broadcasted_iota(
+        jnp.int32, (rows, rows), 1
+    )
+    upto = jnp.where(above, 1.0, 0.0).astype(jnp.bfloat16)
+    last = chip_product((xh_ref, xo_ref), w_ref, chips[3], core)
+    other_first = late if not partner else jnp.logical_not(late)
+    ones = jnp.ones((rows, head_dim), jnp.bfloat16)
+    base_slot = 2 if partner else 0
+    for n, out_ref in enumerate((outh_ref, outo_ref)):
+        query = (acc_ref[base_slot + n] + last[n * rows : (n + 1) * rows]).astype(jnp.bfloat16)
+        self_ref, other_ref = (par_ref, own_ref) if partner else (own_ref, par_ref)
+        sums = []
+        for ref in (lown_ref, lpar_ref, self_ref, other_ref):
+            gates = ref[n, rows : rows + HEAD_PAD, :rows]
+            sums.append(jnp.dot(gates, upto, preferred_element_type=jnp.float32))
+        ends = [s[:, rows - 1 : rows] for s in sums]
+        zero = jnp.zeros_like(ends[0])
+        low_total = ends[0] + ends[1]
+        bases = [
+            jnp.where(late, ends[1], zero),
+            jnp.where(late, zero, ends[0]),
+            low_total + jnp.where(other_first, ends[3], zero),
+            low_total + jnp.where(other_first, zero, ends[2]),
+        ]
+        decay = [s + b for s, b in zip(sums, bases)]
+        query_decay = jnp.transpose(decay[2])
+        shown = (upper, upper, None, other_first)
+        key_decay = [
+            d * log2e if ok is None else jnp.where(ok, d * log2e, FAR) for d, ok in zip(decay, shown)
+        ]
+        blocks = (lown_ref, lpar_ref, self_ref, other_ref)
+        keys = jnp.concatenate([ref[n, :rows, :head_dim] for ref in blocks], axis=0)
+        values = jnp.concatenate(
+            [jnp.concatenate([ref[n, :rows, head_dim:], ones], axis=1) for ref in blocks], axis=0
+        )
+        for head in range(heads):
+            part = query[:, head * head_dim : (head + 1) * head_dim]
+            raw = lax.dot_general(part, keys, NT, preferred_element_type=jnp.float32)
+            pieces = []
+            for i in range(4):
+                piece = raw[:, i * rows : (i + 1) * rows] * (scale * log2e) - key_decay[i][head : head + 1, :]
+                if i == 2:
+                    piece = jnp.where(below, piece, -FAR)
+                pieces.append(piece)
+            top = jnp.maximum(jnp.maximum(pieces[0], pieces[1]), jnp.maximum(pieces[2], pieces[3]))
+            own_decay = query_decay[:, head : head + 1] * log2e
+            row_max = jnp.max(top, axis=1, keepdims=True) + own_decay
+            shift = own_decay - row_max
+            weight = jnp.concatenate(
+                [jnp.exp2(piece + shift).astype(jnp.bfloat16) for piece in pieces], axis=1
+            )
+            sums_out = jnp.dot(weight, values, preferred_element_type=jnp.float32)
+            mixed = sums_out[:, :head_dim] / sums_out[:, head_dim:]
+            out_ref[:, head * head_dim : (head + 1) * head_dim] = mixed.astype(jnp.bfloat16)
+
+
+def attend(partner, scale, acc, xh, xo, weight, blocks):
+    rows, width = xh.shape[0], weight.shape[1]
+    piece = jax.ShapeDtypeStruct((rows, width), jnp.bfloat16)
+    flops = 2 * 2 * rows * 4 * rows * width * 2
+    return pl.pallas_call(
+        functools.partial(attend_kernel, partner, scale),
+        out_shape=(piece, piece),
+        in_specs=[VMEM_SPEC] * 8,
+        out_specs=(VMEM_SPEC, VMEM_SPEC),
+        cost_estimate=pl.CostEstimate(flops=flops, bytes_accessed=acc.size * 4, transcendentals=0),
+        name="attend_partner" if partner else "attend_own",
+    )(acc, xh, xo, weight, *blocks)
+
+
+def place_kernel(a_ref, b_ref, c_ref, d_ref, out_ref):
+    core = lax.rem(lax.axis_index("dp"), 2)
+    half = lax.rem(lax.axis_index("sp"), 2)
+    width = a_ref.shape[1]
+    groups = (2 * half + core, 2 * half + 1 - core, 2 - 2 * half + core, 3 - 2 * half - core)
+    for ref, group in zip((a_ref, b_ref, c_ref, d_ref), groups):
+        out_ref[:, pl.ds(pl.multiple_of(group * width, width), width)] = ref[...]
+
+
+def place(pieces):
+    rows, width = pieces[0].shape
+    return pl.pallas_call(
+        place_kernel,
+        out_shape=jax.ShapeDtypeStruct((rows, 4 * width), jnp.bfloat16),
+        in_specs=[VMEM_SPEC] * 4,
+        out_specs=VMEM_SPEC,
+        name="place",
+    )(*pieces)
+
+
+def paired(tokens, query_weight, key_weight, value_weight, forget_weight, forget_bias):
+    own_home = tokens[0]
+    dp_count, sp_count = lax.axis_size("dp"), lax.axis_size("sp")
+    head_count = forget_weight.shape[1]
+    head_dim = query_weight.shape[1] // head_count
+    group_width = query_weight.shape[1] // sp_count
+    group_heads = head_count // sp_count
+    core = lax.rem(lax.axis_index("dp"), 2)
+    half = lax.rem(lax.axis_index("sp"), 2)
+    swap, hop, turn = core_swap(dp_count), first_hop(dp_count), second_hop(dp_count)
+    partner = [(i, i ^ 1) for i in range(sp_count)]
+    upward = [(i, i + 2) for i in range(sp_count - 2)]
+    across = [
+        (s * dp_count + d, (s ^ 1) * dp_count + (d ^ 1)) for s in range(sp_count) for d in range(dp_count)
+    ]
+
+    def cut(weight, group, width):
+        return lax.dynamic_slice_in_dim(weight, group * width, width, 1)
+
+    def cut_kv(group):
+        return jnp.concatenate(
+            [cut(key_weight, group, head_dim), cut(value_weight, group, head_dim)], axis=1
+        )
+
+    mine, other = 2 * half + core, 2 * half + 1 - core
+    par_home = lax.ppermute(own_home, "sp", partner)
+    kv_0 = jnp.concatenate([cut_kv(mine), lax.ppermute(cut_kv(other), "dp", swap)], axis=0)
+    kv_a = lax.ppermute(kv_0, "dp", hop)
+    kv_b = lax.ppermute(kv_0, "dp", turn)
+    kv_ab = lax.ppermute(kv_a, "dp", turn)
+    q_0 = jnp.concatenate(
+        [
+            cut(query_weight, mine, group_width),
+            lax.ppermute(cut(query_weight, other, group_width), "dp", swap),
+        ],
+        axis=0,
+    )
+    q_a = lax.ppermute(q_0, "dp", hop)
+    q_b = lax.ppermute(q_0, "dp", turn)
+    q_ab = lax.ppermute(q_a, "dp", turn)
+    own_other = lax.ppermute(own_home, "dp", swap)
+    par_other = lax.ppermute(par_home, "dp", swap)
+
+    gate_weight = lax.dynamic_slice_in_dim(forget_weight.T, mine * group_heads, group_heads, 0)
+    gate_weight = jnp.pad(gate_weight, ((0, HEAD_PAD - group_heads), (0, 0)))
+    gate_bias = lax.dynamic_slice_in_dim(forget_bias, mine * group_heads, group_heads, 0)
+    gate_bias = jnp.broadcast_to(
+        jnp.pad(gate_bias, (0, HEAD_PAD - group_heads))[:, None], (HEAD_PAD, 128)
+    )
+
+    kv_weights = (kv_0, kv_a, kv_b, kv_ab)
+    kv_own = project_kv(own_home, own_other, kv_weights, gate_weight, gate_bias)
+    low_own = lax.ppermute(kv_own, "sp", upward)
+    kv_par = project_kv(par_home, par_other, kv_weights, gate_weight, gate_bias)
+    low_par = lax.ppermute(kv_par, "sp", upward)
+    partial = project_q((own_home, own_other, par_home, par_other), (q_0, q_a, q_b))
+    blocks = (kv_own, kv_par, low_own, low_par)
+    scale = head_dim ** (-0.5)
+    out_par_home, out_par_other = attend(True, scale, partial, par_home, par_other, q_ab, blocks)
+    from_across = lax.ppermute(out_par_other, ("sp", "dp"), across)
+    from_partner = lax.ppermute(out_par_home, "sp", partner)
+    out_home, out_other = attend(False, scale, partial, own_home, own_other, q_ab, blocks)
+    from_core = lax.ppermute(out_other, "dp", swap)
+    return place((out_home, from_core, from_partner, from_across))[None]
 
 
 def pick_block(length):
@@ -11,7 +286,7 @@
     return length
 
 
-def on_device(tokens, query_weight, key_weight, value_weight, forget_weight, forget_bias):
+def exchanged(tokens, query_weight, key_weight, value_weight, forget_weight, forget_bias):
     token_rows = tokens[0]
     row_count = token_rows.shape[0]
     sp_count = lax.axis_size("sp")
@@ -121,6 +396,13 @@
     return mixed[None]
 
 
+def on_device(*arrays):
+    key_heads = arrays[2].shape[1] * arrays[4].shape[1] // arrays[1].shape[1]
+    if lax.axis_size("dp") == 8 and lax.axis_size("sp") == 4 and key_heads == 4:
+        return paired(*arrays)
+    return exchanged(*arrays)
+
+
 def solution(mesh):
     placed = (P("dp", "sp", None), P("dp", None), P("dp", None), P("dp", None), P(), P())
     return jax.shard_map(

time: 230 us -> 95.9 us (0.42)
  waiting for transfers between devices: 97 us -> 34.9 us
  matrix products: 27.6 us -> 0 us
  Pallas kernels: 0 us -> 27 us
  local copies, waits for them, and re-layouts: 31.3 us -> 7.36 us
  blocking collectives: 22.2 us -> 0 us
  other arithmetic: 15.3 us -> 0.87 us
  between operations: 13.2 us -> 0.14 us
  starting transfers between devices: 20.2 us -> 25.3 us
  loops' own time: 2.43 us -> 0 us
    all_gather x3 -> x0, waiting for transfers between devices: 89.3 us -> none  [the longest x1 48.7 us: on_device(): lax.all_gather(query_weight, 'dp', axis=0, tiled=True)]
    ppermute x0 -> x16, waiting for transfers between devices: none -> 34.9 us  [the longest x1 12.6 us: paired(): par_home = lax.ppermute(own_home, 'sp', partner)]
    dot_general x10 -> x0, matrix products: 27.6 us -> none  [the longest x3 10.8 us: weighted(): jnp.einsum('kgqs,skd->qkgd', weights, value_part, preferred_element_type=...]
    pallas_call x0 -> x6, Pallas kernels: none -> 27 us  [the longest x2 13.3 us: attend(): pl.pallas_call(functools.partial(attend_kernel, partner, scale), out_shap...]
    ppermute x0 -> x16, starting transfers between devices: none -> 25.3 us  [the longest x1 7.13 us: paired(): from_partner = lax.ppermute(out_par_home, 'sp', partner)]
    all_to_all x1 -> x0, blocking collectives: 22.2 us -> none  [on_device(): lax.all_to_all(head_mixed, 'sp', split_axis=0, concat_axis=1, tiled=True)]
    all_to_all x4 -> x0, starting transfers between devices: 20.1 us -> none  [the longest x1 6.35 us: on_device(): lax.all_to_all(log_gate, 'sp', split_axis=1, concat_axis=0, tiled=True)]
    dynamic_slice x14 -> x4, local copies, waits for them, and re-layouts: 15 us -> 2.12 us  [the longest x2 2.04 us: cut(): return lax.dynamic_slice_in_dim(weight, group * width, width, 1)]
  transfers between devices with their start and end apart: 7 -> 16, of which waited for: 4 -> 5; matrix products, arithmetic and copies ran while one was open for 7% -> 5% of each run, Pallas kernels for 0% -> 19%
where the time goes in v1:
time: 95.9 us; the launch traced here: 95.6 us
  waiting for transfers between devices  34.9 us (36%)
  Pallas kernels  27 us (28%)
  starting transfers between devices  25.3 us (26%)
  local copies, waits for them, and re-layouts  7.36 us (8%)
    pallas_call x2, Pallas kernels, attend(): pl.pallas_call(functools.partial(attend_kernel, partner, scale), out_shap...  13.3 us
    ppermute x1, waiting for transfers between devices, paired(): par_home = lax.ppermute(own_home, 'sp', partner)  12.6 us
    ppermute x1, waiting for transfers between devices, paired(): kv_ab = lax.ppermute(kv_a, 'dp', turn)  7.53 us
    ppermute x1, starting transfers between devices, paired(): from_partner = lax.ppermute(out_par_home, 'sp', partner)  7.13 us
    pallas_call x2, Pallas kernels, project_kv(): pl.pallas_call(kv_kernel, out_shape=jax.ShapeDtypeStruct((2, rows + GATE_...  6.64 us
    ppermute x1, waiting for transfers between devices, paired(): from_partner = lax.ppermute(out_par_home, 'sp', partner)  5.85 us
    ppermute x1, waiting for transfers between devices, paired(): kv_a = lax.ppermute(kv_0, 'dp', hop)  5.06 us
    pallas_call x1, Pallas kernels, project_q(): pl.pallas_call(q_kernel, out_shape=jax.ShapeDtypeStruct((4, rows, width),...  4.89 us
  transfers between devices with their start and end apart: 16, of which 5 were waited for; matrix products, arithmetic and copies ran while one was open for 5% of the time, Pallas kernels for 19%

profile of v1, /device:TPU:0, one launch (start us, length us, event | category | flops | bytes accessed | tf_op | source)
XLA Modules:
  0.0 95.6 jit_solution(5388932814665146579)
XLA Ops:
  0.0 0.0 copy-start
  0.0 3.1 %collective-permute-start.1 = (bf16[192,2048]{1,0:T(8,128)(2,1)}, bf16[192,2048]{1,0:T(8,128)(2,1)S(1)}, u32[]{:S(2)}, u32[]{:S(2)}) collective-permute-start(bf16[192,2048]{1,0:T(8,128)(2,1)} %bitcast.4), channel_id=1, source_target_pairs={{0,8},{8,0},{16,24},{24,16},{1,9},{9,1},{17,25},{25,17},{2,10},{10... | collective-permute-start | bytes 2359304 | tf_op jit(solution)/shard_map/ppermute | solution.py:241
  3.1 0.0 copy-start.13
  3.1 1.1 %constant_dynamic-slice_fusion.5 = (bf16[256,512]{1,0:T(8,128)(2,1)S(1)}, bf16[256,512]{1,0:T(8,128)(2,1)S(1)}) fusion(bf16[256,2048]{1,0:T(8,128)(2,1)} %param.7, s32[]{:T(128)S(6)} %select_n.18, s32[]{:T(128)S(6)} %select_n.19), kind=kLoop, calls=%fused_computation.9 | loop fusion | bytes 1048584 | tf_op jit(solution)/shard_map/dynamic_slice | solution.py:233
  4.1 0.1 collective-permute-start.3
  4.2 0.5 collective-permute-start
  4.7 1.0 %constant_dynamic-slice_fusion.2 = (bf16[256,128]{1,0:T(8,128)(2,1)S(1)}, bf16[256,128]{1,0:T(8,128)(2,1)S(1)}, bf16[256,128]{1,0:T(8,128)(2,1)S(1)}, bf16[256,128]{1,0:T(8,128)(2,1)S(1)}) fusion(bf16[256,512]{1,0:T(8,128)(2,1)} %param.9, s32[]{:T(128)S(6)} %select_n.20, s32[]{:T(128)S(6)} %select_n.21, bf16[256,512]{1,0:T(8,128)(2,1)} %param.8), kind=kLoop, calls=%fused_computation.6 | loop fusion | bytes 524296 | tf_op jit(solution)/shard_map/dynamic_slice | solution.py:233
  5.7 0.1 collective-permute-start.7
  5.8 0.0 collective-permute-done.3
  5.8 0.8 pad_maximum_fusion.w0_ref
  6.7 1.5 %collective-permute-start.4 = (bf16[512,512]{1,0:T(8,128)(2,1)}, bf16[512,512]{1,0:T(8,128)(2,1)}, u32[]{:S(2)}, u32[]{:S(2)}) collective-permute-start(bf16[512,512]{1,0:T(8,128)(2,1)} %pad_maximum_fusion.w0_ref), channel_id=1, source_target_pairs={{0,2},{1,5},{2,0},{3,7},{4,6},{5,1},{6,4},{7,3},{8,10},{9,13},{10,... | collective-permute-start | bytes 1572872 | tf_op jit(solution)/shard_map/ppermute | solution.py:253
  8.2 12.6 %collective-permute-done.1.xc_ref.xh_ref = bf16[192,2048]{1,0:T(8,128)(2,1)S(1)} collective-permute-done((bf16[192,2048]{1,0:T(8,128)(2,1)}, bf16[192,2048]{1,0:T(8,128)(2,1)S(1)}, u32[]{:S(2)}, u32[]{:S(2)}) %collective-permute-start.1) | collective-permute-done | bytes 786464 | tf_op jit(solution)/shard_map/ppermute | solution.py:241
  20.8 0.0 copy-start.1
  20.8 0.0 collective-permute-start.2
  20.8 0.0 collective-permute-done.7
  20.8 0.0 copy-start.4
  20.9 1.7 %collective-permute-start.8 = (bf16[512,256]{1,0:T(8,128)(2,1)S(1)}, bf16[512,256]{1,0:T(8,128)(2,1)S(1)}, u32[]{:S(2)}, u32[]{:S(2)}) collective-permute-start(bf16[512,256]{1,0:T(8,128)(2,1)S(1)} %pad_maximum_fusion.1.w0_ref), channel_id=1, source_target_pairs={{0,2},{1,5},{2,0},{3,7},{4,6},{5,1},{6,4},{7,3},{8,10},{9,13},{10,... | collective-permute-start | bytes 786440 | tf_op jit(solution)/shard_map/ppermute | solution.py:243
  22.6 1.5 %collective-permute-start.9 = (bf16[512,256]{1,0:T(8,128)(2,1)S(1)}, bf16[512,256]{1,0:T(8,128)(2,1)S(1)}, u32[]{:S(2)}, u32[]{:S(2)}) collective-permute-start(bf16[512,256]{1,0:T(8,128)(2,1)S(1)} %pad_maximum_fusion.1.w0_ref), channel_id=1, source_target_pairs={{0,4},{1,3},{2,6},{3,1},{4,0},{5,7},{6,2},{7,5},{8,12},{9,11},{10,... | collective-permute-start | bytes 786440 | tf_op jit(solution)/shard_map/ppermute | solution.py:244
  24.1 5.1 %collective-permute-done.8.wa_ref = bf16[512,256]{1,0:T(8,128)(2,1)S(1)} collective-permute-done((bf16[512,256]{1,0:T(8,128)(2,1)S(1)}, bf16[512,256]{1,0:T(8,128)(2,1)S(1)}, u32[]{:S(2)}, u32[]{:S(2)}) %collective-permute-start.8) | collective-permute-done | bytes 262176 | tf_op jit(solution)/shard_map/ppermute | solution.py:243
  29.2 2.2 %collective-permute-start.5 = (bf16[512,512]{1,0:T(8,128)(2,1)}, bf16[512,512]{1,0:T(8,128)(2,1)}, u32[]{:S(2)}, u32[]{:S(2)}) collective-permute-start(bf16[512,512]{1,0:T(8,128)(2,1)} %pad_maximum_fusion.w0_ref), channel_id=1, source_target_pairs={{0,4},{1,3},{2,6},{3,1},{4,0},{5,7},{6,2},{7,5},{8,12},{9,11},{10,... | collective-permute-start | bytes 1572872 | tf_op jit(solution)/shard_map/ppermute | solution.py:254
  31.4 0.0 collective-permute-done.9.wb_ref
  31.4 0.1 collective-permute-start.10
  31.5 0.6 copy-done.7
  32.1 0.0 collective-permute-done.4.wa_ref
  32.1 1.3 %collective-permute-start.6 = (bf16[512,512]{1,0:T(8,128)(2,1)}, bf16[512,512]{1,0:T(8,128)(2,1)S(1)}, u32[]{:S(2)}, u32[]{:S(2)}) collective-permute-start(bf16[512,512]{1,0:T(8,128)(2,1)} %collective-permute-done.4.wa_ref), channel_id=1, source_target_pairs={{0,4},{1,3},{2,6},{3,1},{4,0},{5,7},{6,2},{7,5},{8,12},{9,11},{10,... | collective-permute-start | bytes 1572872 | tf_op jit(solution)/shard_map/ppermute | solution.py:255
  33.4 0.0 copy-done.13
  33.4 0.1 dynamic_slice.31
  33.5 0.0 copy-done
  33.5 0.6 pad.8.wf_ref
  34.2 7.5 %collective-permute-done.10.wab_ref = bf16[512,256]{1,0:T(8,128)(2,1)} collective-permute-done((bf16[512,256]{1,0:T(8,128)(2,1)S(1)}, bf16[512,256]{1,0:T(8,128)(2,1)}, u32[]{:S(2)}, u32[]{:S(2)}) %collective-permute-start.10) | collective-permute-done | bytes 262176 | tf_op jit(solution)/shard_map/ppermute | solution.py:245
  41.7 0.0 collective-permute-done.xb_ref.xo_ref
  41.7 0.7 broadcast_in_dim.4.bias_ref
  42.4 0.0 copy-done.4
  42.4 0.0 copy-done.6
  42.4 0.1 copy-done.2
  42.6 3.3 %project_kv.2.own_ref = bf16[2,208,256]{2,1,0:T(8,128)(2,1)} custom-call(bf16[192,2048]{1,0:T(8,128)(2,1)} %bitcast.6, bf16[192,2048]{1,0:T(8,128)(2,1)} %copy-done.2, bf16[512,256]{1,0:T(8,128)(2,1)} %copy-done.4, bf16[512,256]{1,0:T(8,128)(2,1)} %copy-done.6, bf16[512,256]{1,0:T(8,128)(2,1)} %copy-done.7, ...), custom_call_target="tpu_custom_call" | custom-call | flops 402653184 | bytes 1572864 | tf_op jit(solution)/shard_map/project_kv/pallas_call | solution.py:78
  45.9 0.0 copy-done.1
  45.9 4.6 %collective-permute-start.11 = (bf16[2,208,256]{2,1,0:T(8,128)(2,1)}, bf16[2,208,256]{2,1,0:T(8,128)(2,1)S(1)}, u32[]{:S(2)}, u32[]{:S(2)}) collective-permute-start(bf16[2,208,256]{2,1,0:T(8,128)(2,1)} %project_kv.2.own_ref), channel_id=1, source_target_pairs={{0,16},{8,24},{1,17},{9,25},{2,18},{10,26},{3,19},{11,27},{4,20},{... | collective-permute-start | bytes 638984 | tf_op jit(solution)/shard_map/ppermute | solution.py:268
  50.5 0.0 collective-permute-done.2.xd_ref.xo_ref
  50.5 0.0 copy-start.3
  50.6 0.9 copy-done.3
  51.4 3.3 %project_kv.3.par_ref = bf16[2,208,256]{2,1,0:T(8,128)(2,1)} custom-call(bf16[192,2048]{1,0:T(8,128)(2,1)} %copy-done.1, bf16[192,2048]{1,0:T(8,128)(2,1)} %copy-done.3, bf16[512,256]{1,0:T(8,128)(2,1)} %copy-done.4, bf16[512,256]{1,0:T(8,128)(2,1)} %copy-done.6, bf16[512,256]{1,0:T(8,128)(2,1)} %copy-done.7, ...), custom_call_target="tpu_custom_call" | custom-call | flops 402653184 | bytes 1572864 | tf_op jit(solution)/shard_map/project_kv/pallas_call | solution.py:78
  54.8 1.3 %collective-permute-start.12 = (bf16[2,208,256]{2,1,0:T(8,128)(2,1)}, bf16[2,208,256]{2,1,0:T(8,128)(2,1)S(1)}, u32[]{:S(2)}, u32[]{:S(2)}) collective-permute-start(bf16[2,208,256]{2,1,0:T(8,128)(2,1)} %project_kv.3.par_ref), channel_id=1, source_target_pairs={{0,16},{8,24},{1,17},{9,25},{2,18},{10,26},{3,19},{11,27},{4,20},{... | collective-permute-start | bytes 638984 | tf_op jit(solution)/shard_map/ppermute | solution.py:270
  56.1 0.0 collective-permute-done.5.wb_ref
  56.1 4.9 %project_q.1.acc_ref = f32[4,192,512]{2,1,0:T(8,128)} custom-call(bf16[192,2048]{1,0:T(8,128)(2,1)} %bitcast.7, bf16[192,2048]{1,0:T(8,128)(2,1)} %copy-done.2, bf16[192,2048]{1,0:T(8,128)(2,1)} %copy-done.1, bf16[192,2048]{1,0:T(8,128)(2,1)} %copy-done.3, bf16[512,512]{1,0:T(8,128)(2,1)} %pad_maximum_fusion.w0_ref, ...), custom_call_target="tpu_custom_call" | custom-call | flops 1207959552 | bytes 3145728 | tf_op jit(solution)/shard_map/project_q/pallas_call | solution.py:102
  61.0 0.0 collective-permute-done.11.lown_ref
  61.0 0.0 collective-permute-done.6.w_ref
  61.0 0.0 copy-start.5
  61.0 0.0 collective-permute-done.12.lpar_ref
  61.0 0.6 copy-done.8
  61.6 0.2 copy-done.5
  61.8 0.7 copy-done.9
  62.5 6.7 %attend_own.1 = (bf16[192,512]{1,0:T(8,128)(2,1)}, bf16[192,512]{1,0:T(8,128)(2,1)}) custom-call(f32[4,192,512]{2,1,0:T(8,128)} %project_q.1.acc_ref, bf16[192,2048]{1,0:T(8,128)(2,1)} %bitcast.8, bf16[192,2048]{1,0:T(8,128)(2,1)} %copy-done.2, bf16[512,512]{1,0:T(8,128)(2,1)} %copy-done.5, bf16[2,208,256]{2,1,0:T(8,128)(2,1)} %project_kv.2.own_ref, ...), custom_call_target="tpu_custom_call" | custom-call | flops 603979776 | bytes 1572864 | tf_op jit(solution)/shard_map/attend_own/pallas_call | solution.py:186
  69.2 0.0 collective-permute-start.13
  69.2 6.7 %attend_partner.1 = (bf16[192,512]{1,0:T(8,128)(2,1)}, bf16[192,512]{1,0:T(8,128)(2,1)}) custom-call(f32[4,192,512]{2,1,0:T(8,128)} %project_q.1.acc_ref, bf16[192,2048]{1,0:T(8,128)(2,1)} %copy-done.1, bf16[192,2048]{1,0:T(8,128)(2,1)} %copy-done.3, bf16[512,512]{1,0:T(8,128)(2,1)} %copy-done.5, bf16[2,208,256]{2,1,0:T(8,128)(2,1)} %project_kv.2.own_ref, ...), custom_call_target="tpu_custom_call" | custom-call | flops 603979776 | bytes 1572864 | tf_op jit(solution)/shard_map/attend_partner/pallas_call | solution.py:186
  75.8 7.1 %collective-permute-start.14 = (bf16[192,512]{1,0:T(8,128)(2,1)}, bf16[192,512]{1,0:T(8,128)(2,1)S(1)}, u32[]{:S(2)}, u32[]{:S(2)}) collective-permute-start(bf16[192,512]{1,0:T(8,128)(2,1)} %get-tuple-element.11), channel_id=1, source_target_pairs={{0,8},{8,0},{16,24},{24,16},{1,9},{9,1},{17,25},{25,17},{2,10},{10... | collective-permute-start | bytes 589832 | tf_op jit(solution)/shard_map/ppermute | solution.py:276
  83.0 0.1 collective-permute-start.15
  83.1 0.0 collective-permute-done.13.b_ref
  83.1 5.8 %collective-permute-done.14.c_ref = bf16[192,512]{1,0:T(8,128)(2,1)S(1)} collective-permute-done((bf16[192,512]{1,0:T(8,128)(2,1)}, bf16[192,512]{1,0:T(8,128)(2,1)S(1)}, u32[]{:S(2)}, u32[]{:S(2)}) %collective-permute-start.14) | collective-permute-done | bytes 196640 | tf_op jit(solution)/shard_map/ppermute | solution.py:276
  88.9 3.8 %collective-permute-done.15.d_ref = bf16[192,512]{1,0:T(8,128)(2,1)S(1)} collective-permute-done((bf16[192,512]{1,0:T(8,128)(2,1)}, bf16[192,512]{1,0:T(8,128)(2,1)S(1)}, u32[]{:S(2)}, u32[]{:S(2)}) %collective-permute-start.15) | collective-permute-done | bytes 196640 | tf_op jit(solution)/shard_map/ppermute | solution.py:275
  92.8 0.0 copy-done.10
  92.8 0.0 copy-done.11
  92.8 0.7 copy-done.12
  93.4 2.2 %place.1 = bf16[192,2048]{1,0:T(8,128)(2,1)} custom-call(bf16[192,512]{1,0:T(8,128)(2,1)} %get-tuple-element.9.a_ref, bf16[192,512]{1,0:T(8,128)(2,1)} %copy-done.10, bf16[192,512]{1,0:T(8,128)(2,1)} %copy-done.11, bf16[192,512]{1,0:T(8,128)(2,1)} %copy-done.12), custom_call_target="tpu_custom_call" | custom-call | tf_op jit(solution)/shard_map/place/pallas_call | solution.py:207
  (12 shorter events, 0.1 us)
Async XLA Ops:
  0.0 33.5 %copy-start = (bf16[2048,16]{0,1:T(8,128)(2,1)S(1)}, bf16[2048,16]{0,1:T(8,128)(2,1)}, u32[]{:S(2)}) copy-start(bf16[2048,16]{0,1:T(8,128)(2,1)} %param.10) | copy-start | bytes 196612
  0.0 20.8 %collective-permute-start.1 = (bf16[192,2048]{1,0:T(8,128)(2,1)}, bf16[192,2048]{1,0:T(8,128)(2,1)S(1)}, u32[]{:S(2)}, u32[]{:S(2)}) collective-permute-start(bf16[192,2048]{1,0:T(8,128)(2,1)} %bitcast.4), channel_id=1, source_target_pairs={{0,8},{8,0},{16,24},{24,16},{1,9},{9,1},{17,25},{25,17},{2,10},{10... | collective-permute-start | bytes 2359304 | tf_op jit(solution)/shard_map/ppermute | solution.py:241
  3.1 30.4 %copy-start.13 = (f32[16]{0:T(128)S(1)}, f32[16]{0:T(128)}, u32[]{:S(2)}) copy-start(f32[16]{0:T(128)} %param.11) | copy-start | bytes 196
  4.1 1.7 %collective-permute-start.3 = (bf16[256,512]{1,0:T(8,128)(2,1)S(1)}, bf16[256,512]{1,0:T(8,128)(2,1)S(1)}, u32[]{:S(2)}, u32[]{:S(2)}) collective-permute-start(bf16[256,512]{1,0:T(8,128)(2,1)S(1)} %get-tuple-element.14), channel_id=1, source_target_pairs={{0,1},{1,0},{2,3},{3,2},{4,5},{5,4},{6,7},{7,6},{8,9},{9,8},{10,11... | collective-permute-start | bytes 786440 | tf_op jit(solution)/shard_map/ppermute | solution.py:249
  4.2 37.5 %collective-permute-start = (bf16[192,2048]{1,0:T(8,128)(2,1)}, bf16[192,2048]{1,0:T(8,128)(2,1)S(1)}, u32[]{:S(2)}, u32[]{:S(2)}) collective-permute-start(bf16[192,2048]{1,0:T(8,128)(2,1)} %bitcast.5), channel_id=1, source_target_pairs={{0,1},{1,0},{2,3},{3,2},{4,5},{5,4},{6,7},{7,6},{8,9},{9,8},{10,11... | collective-permute-start | bytes 2359304 | tf_op jit(solution)/shard_map/ppermute | solution.py:256
  5.7 15.1 %collective-permute-start.7 = (bf16[256,256]{1,0:T(8,128)(2,1)S(1)}, bf16[256,256]{1,0:T(8,128)(2,1)S(1)}, u32[]{:S(2)}, u32[]{:S(2)}) collective-permute-start(bf16[256,256]{1,0:T(8,128)(2,1)S(1)} %pad_maximum_fusion.2), channel_id=1, source_target_pairs={{0,1},{1,0},{2,3},{3,2},{4,5},{5,4},{6,7},{7,6},{8,9},{9,8},{10,11... | collective-permute-start | bytes 393224 | tf_op jit(solution)/shard_map/ppermute | solution.py:242
  6.7 25.4 %collective-permute-start.4 = (bf16[512,512]{1,0:T(8,128)(2,1)}, bf16[512,512]{1,0:T(8,128)(2,1)}, u32[]{:S(2)}, u32[]{:S(2)}) collective-permute-start(bf16[512,512]{1,0:T(8,128)(2,1)} %pad_maximum_fusion.w0_ref), channel_id=1, source_target_pairs={{0,2},{1,5},{2,0},{3,7},{4,6},{5,1},{6,4},{7,3},{8,10},{9,13},{10,... | collective-permute-start | bytes 1572872 | tf_op jit(solution)/shard_map/ppermute | solution.py:253
  20.8 25.1 %copy-start.1 = (bf16[192,2048]{1,0:T(8,128)(2,1)}, bf16[192,2048]{1,0:T(8,128)(2,1)S(1)}, u32[]{:S(2)}) copy-start(bf16[192,2048]{1,0:T(8,128)(2,1)S(1)} %collective-permute-done.1.xc_ref.xh_ref) | copy-start | bytes 2359300
  20.8 29.7 %collective-permute-start.2 = (bf16[192,2048]{1,0:T(8,128)(2,1)S(1)}, bf16[192,2048]{1,0:T(8,128)(2,1)S(1)}, u32[]{:S(2)}, u32[]{:S(2)}) collective-permute-start(bf16[192,2048]{1,0:T(8,128)(2,1)S(1)} %collective-permute-done.1.xc_ref.xh_ref), channel_id=1, source_target_pairs={{0,1},{1,0},{2,3},{3,2},{4,5},{5,4},{6,7},{7,6},{8,9},{9,8},{10,11... | collective-permute-start | bytes 2359304 | tf_op jit(solution)/shard_map/ppermute | solution.py:257
  20.8 21.6 %copy-start.4 = (bf16[512,256]{1,0:T(8,128)(2,1)}, bf16[512,256]{1,0:T(8,128)(2,1)S(1)}, u32[]{:S(2)}) copy-start(bf16[512,256]{1,0:T(8,128)(2,1)S(1)} %pad_maximum_fusion.1.w0_ref) | copy-start | bytes 786436
  20.9 8.3 %collective-permute-start.8 = (bf16[512,256]{1,0:T(8,128)(2,1)S(1)}, bf16[512,256]{1,0:T(8,128)(2,1)S(1)}, u32[]{:S(2)}, u32[]{:S(2)}) collective-permute-start(bf16[512,256]{1,0:T(8,128)(2,1)S(1)} %pad_maximum_fusion.1.w0_ref), channel_id=1, source_target_pairs={{0,2},{1,5},{2,0},{3,7},{4,6},{5,1},{6,4},{7,3},{8,10},{9,13},{10,... | collective-permute-start | bytes 786440 | tf_op jit(solution)/shard_map/ppermute | solution.py:243
  22.6 8.8 %collective-permute-start.9 = (bf16[512,256]{1,0:T(8,128)(2,1)S(1)}, bf16[512,256]{1,0:T(8,128)(2,1)S(1)}, u32[]{:S(2)}, u32[]{:S(2)}) collective-permute-start(bf16[512,256]{1,0:T(8,128)(2,1)S(1)} %pad_maximum_fusion.1.w0_ref), channel_id=1, source_target_pairs={{0,4},{1,3},{2,6},{3,1},{4,0},{5,7},{6,2},{7,5},{8,12},{9,11},{10,... | collective-permute-start | bytes 786440 | tf_op jit(solution)/shard_map/ppermute | solution.py:244
  29.2 13.3 %copy-start.6 = (bf16[512,256]{1,0:T(8,128)(2,1)}, bf16[512,256]{1,0:T(8,128)(2,1)S(1)}, u32[]{:S(2)}) copy-start(bf16[512,256]{1,0:T(8,128)(2,1)S(1)} %collective-permute-done.8.wa_ref) | copy-start | bytes 786436
  29.2 26.9 %collective-permute-start.5 = (bf16[512,512]{1,0:T(8,128)(2,1)}, bf16[512,512]{1,0:T(8,128)(2,1)}, u32[]{:S(2)}, u32[]{:S(2)}) collective-permute-start(bf16[512,512]{1,0:T(8,128)(2,1)} %pad_maximum_fusion.w0_ref), channel_id=1, source_target_pairs={{0,4},{1,3},{2,6},{3,1},{4,0},{5,7},{6,2},{7,5},{8,12},{9,11},{10,... | collective-permute-start | bytes 1572872 | tf_op jit(solution)/shard_map/ppermute | solution.py:254
  31.4 0.7 copy-start.7
  31.4 10.3 %collective-permute-start.10 = (bf16[512,256]{1,0:T(8,128)(2,1)S(1)}, bf16[512,256]{1,0:T(8,128)(2,1)}, u32[]{:S(2)}, u32[]{:S(2)}) collective-permute-start(bf16[512,256]{1,0:T(8,128)(2,1)S(1)} %collective-permute-done.8.wa_ref), channel_id=1, source_target_pairs={{0,4},{1,3},{2,6},{3,1},{4,0},{5,7},{6,2},{7,5},{8,12},{9,11},{10,... | collective-permute-start | bytes 786440 | tf_op jit(solution)/shard_map/ppermute | solution.py:245
  32.1 28.8 %collective-permute-start.6 = (bf16[512,512]{1,0:T(8,128)(2,1)}, bf16[512,512]{1,0:T(8,128)(2,1)S(1)}, u32[]{:S(2)}, u32[]{:S(2)}) collective-permute-start(bf16[512,512]{1,0:T(8,128)(2,1)} %collective-permute-done.4.wa_ref), channel_id=1, source_target_pairs={{0,4},{1,3},{2,6},{3,1},{4,0},{5,7},{6,2},{7,5},{8,12},{9,11},{10,... | collective-permute-start | bytes 1572872 | tf_op jit(solution)/shard_map/ppermute | solution.py:255
  41.7 0.9 copy-start.2
  45.9 15.1 %collective-permute-start.11 = (bf16[2,208,256]{2,1,0:T(8,128)(2,1)}, bf16[2,208,256]{2,1,0:T(8,128)(2,1)S(1)}, u32[]{:S(2)}, u32[]{:S(2)}) collective-permute-start(bf16[2,208,256]{2,1,0:T(8,128)(2,1)} %project_kv.2.own_ref), channel_id=1, source_target_pairs={{0,16},{8,24},{1,17},{9,25},{2,18},{10,26},{3,19},{11,27},{4,20},{... | collective-permute-start | bytes 638984 | tf_op jit(solution)/shard_map/ppermute | solution.py:268
  50.5 0.9 copy-start.3
  54.8 6.2 %collective-permute-start.12 = (bf16[2,208,256]{2,1,0:T(8,128)(2,1)}, bf16[2,208,256]{2,1,0:T(8,128)(2,1)S(1)}, u32[]{:S(2)}, u32[]{:S(2)}) collective-permute-start(bf16[2,208,256]{2,1,0:T(8,128)(2,1)} %project_kv.3.par_ref), channel_id=1, source_target_pairs={{0,16},{8,24},{1,17},{9,25},{2,18},{10,26},{3,19},{11,27},{4,20},{... | collective-permute-start | bytes 638984 | tf_op jit(solution)/shard_map/ppermute | solution.py:270
  61.0 0.7 copy-start.8
  61.0 0.9 copy-start.5
  61.8 0.7 copy-start.9
  69.2 13.9 %collective-permute-start.13 = (bf16[192,512]{1,0:T(8,128)(2,1)}, bf16[192,512]{1,0:T(8,128)(2,1)S(1)}, u32[]{:S(2)}, u32[]{:S(2)}) collective-permute-start(bf16[192,512]{1,0:T(8,128)(2,1)} %get-tuple-element.10), channel_id=1, source_target_pairs={{0,1},{1,0},{2,3},{3,2},{4,5},{5,4},{6,7},{7,6},{8,9},{9,8},{10,11... | collective-permute-start | bytes 589832 | tf_op jit(solution)/shard_map/ppermute | solution.py:278
  75.8 13.1 %collective-permute-start.14 = (bf16[192,512]{1,0:T(8,128)(2,1)}, bf16[192,512]{1,0:T(8,128)(2,1)S(1)}, u32[]{:S(2)}, u32[]{:S(2)}) collective-permute-start(bf16[192,512]{1,0:T(8,128)(2,1)} %get-tuple-element.11), channel_id=1, source_target_pairs={{0,8},{8,0},{16,24},{24,16},{1,9},{9,1},{17,25},{25,17},{2,10},{10... | collective-permute-start | bytes 589832 | tf_op jit(solution)/shard_map/ppermute | solution.py:276
  83.0 9.8 %collective-permute-start.15 = (bf16[192,512]{1,0:T(8,128)(2,1)}, bf16[192,512]{1,0:T(8,128)(2,1)S(1)}, u32[]{:S(2)}, u32[]{:S(2)}) collective-permute-start(bf16[192,512]{1,0:T(8,128)(2,1)} %get-tuple-element.12), channel_id=1, source_target_pairs={{0,9},{1,8},{2,11},{3,10},{4,13},{5,12},{6,15},{7,14},{8,1},{9,0},... | collective-permute-start | bytes 589832 | tf_op jit(solution)/shard_map/ppermute | solution.py:275
  83.1 9.7 %copy-start.10 = (bf16[192,512]{1,0:T(8,128)(2,1)}, bf16[192,512]{1,0:T(8,128)(2,1)S(1)}, u32[]{:S(2)}) copy-start(bf16[192,512]{1,0:T(8,128)(2,1)S(1)} %collective-permute-done.13.b_ref) | copy-start | bytes 589828
  88.9 3.8 %copy-start.11 = (bf16[192,512]{1,0:T(8,128)(2,1)}, bf16[192,512]{1,0:T(8,128)(2,1)S(1)}, u32[]{:S(2)}) copy-start(bf16[192,512]{1,0:T(8,128)(2,1)S(1)} %collective-permute-done.14.c_ref) | copy-start | bytes 589828
  92.8 0.7 copy-start.12

commit v2 on v1

--- a/solution.py
+++ b/solution.py
@@ -8,7 +8,9 @@
 from jax.experimental.pallas import tpu as pltpu
 from jax.sharding import PartitionSpec as P
 
+
 VMEM_SPEC = pl.BlockSpec(memory_space=pltpu.VMEM)
+KEEP_ROOM = pltpu.CompilerParams(vmem_limit_bytes=24 * 1024 * 1024)
 FAR = 1e30
 GATE_ROWS = 16
 HEAD_PAD = 8
@@ -54,9 +56,26 @@
     return total
 
 
+def group_rows(stacked, group, size):
+    parts = [
+        jnp.concatenate([stacked[i * size : (i + 1) * size]] * (HEAD_PAD // size), axis=0)
+        for i in range(stacked.shape[0] // size)
+    ]
+    chosen = parts[0]
+    for i, part in enumerate(parts[1:], 1):
+        chosen = jnp.where(group == i, part, chosen)
+    return chosen
+
+
 def kv_kernel(xh_ref, xo_ref, w0_ref, wa_ref, wb_ref, wab_ref, wf_ref, bias_ref, out_ref):
     core, chips = chip_sources()
+    group = 2 * lax.rem(lax.axis_index("sp"), 2) + core
     rows = xh_ref.shape[0]
+    group_heads = wf_ref.shape[0] // 4
+    head_row = lax.broadcasted_iota(jnp.int32, (HEAD_PAD, rows), 0)
+    bias = jnp.zeros((HEAD_PAD, rows), jnp.float32)
+    for i in range(group_heads):
+        bias = jnp.where(head_row == i, bias_ref[group * group_heads + i], bias)
     total = None
     for chip, weight_ref in zip(chips, (w0_ref, wa_ref, wb_ref, wab_ref)):
         term = chip_product((xh_ref, xo_ref), weight_ref, chip, core)
@@ -64,7 +83,7 @@
     for n, x_ref in enumerate((xh_ref, xo_ref)):
         out_ref[n, :rows, :] = total[n * rows : (n + 1) * rows].astype(jnp.bfloat16)
         logit = lax.dot_general(wf_ref[...], x_ref[...], NT, preferred_element_type=jnp.float32)
-        logit = logit + bias_ref[:, 0:1]
+        logit = group_rows(logit, group, group_heads) + bias
         gate = jnp.minimum(logit, 0.0) - jnp.log1p(jnp.exp(-jnp.abs(logit)))
         pad = out_ref.shape[2] - rows
         wide = jnp.concatenate([gate, jnp.zeros((HEAD_PAD, pad), jnp.float32)], axis=1)
@@ -78,9 +97,10 @@
     return pl.pallas_call(
         kv_kernel,
         out_shape=jax.ShapeDtypeStruct((2, rows + GATE_ROWS, width), jnp.bfloat16),
-        in_specs=[VMEM_SPEC] * 8,
+        in_specs=[VMEM_SPEC] * 7 + [pl.BlockSpec(memory_space=pltpu.SMEM)],
         out_specs=VMEM_SPEC,
         cost_estimate=pl.CostEstimate(flops=flops, bytes_accessed=2 * xh.size * 2, transcendentals=0),
+        compiler_params=KEEP_ROOM,
         name="project_kv",
     )(xh, xo, *weights, wf, bias)
 
@@ -105,6 +125,7 @@
         in_specs=[VMEM_SPEC] * 7,
         out_specs=VMEM_SPEC,
         cost_estimate=pl.CostEstimate(flops=flops, bytes_accessed=4 * xs[0].size * 2, transcendentals=0),
+        compiler_params=KEEP_ROOM,
         name="project_q",
     )(*xs, *weights)
 
@@ -189,6 +210,7 @@
         in_specs=[VMEM_SPEC] * 8,
         out_specs=(VMEM_SPEC, VMEM_SPEC),
         cost_estimate=pl.CostEstimate(flops=flops, bytes_accessed=acc.size * 4, transcendentals=0),
+        compiler_params=KEEP_ROOM,
         name="attend_partner" if partner else "attend_own",
     )(acc, xh, xo, weight, *blocks)
 
@@ -209,6 +231,7 @@
         out_shape=jax.ShapeDtypeStruct((rows, 4 * width), jnp.bfloat16),
         in_specs=[VMEM_SPEC] * 4,
         out_specs=VMEM_SPEC,
+        compiler_params=KEEP_ROOM,
         name="place",
     )(*pieces)
 
@@ -219,7 +242,6 @@
     head_count = forget_weight.shape[1]
     head_dim = query_weight.shape[1] // head_count
     group_width = query_weight.shape[1] // sp_count
-    group_heads = head_count // sp_count
     core = lax.rem(lax.axis_index("dp"), 2)
     half = lax.rem(lax.axis_index("sp"), 2)
     swap, hop, turn = core_swap(dp_count), first_hop(dp_count), second_hop(dp_count)
@@ -256,17 +278,10 @@
     own_other = lax.ppermute(own_home, "dp", swap)
     par_other = lax.ppermute(par_home, "dp", swap)
 
-    gate_weight = lax.dynamic_slice_in_dim(forget_weight.T, mine * group_heads, group_heads, 0)
-    gate_weight = jnp.pad(gate_weight, ((0, HEAD_PAD - group_heads), (0, 0)))
-    gate_bias = lax.dynamic_slice_in_dim(forget_bias, mine * group_heads, group_heads, 0)
-    gate_bias = jnp.broadcast_to(
-        jnp.pad(gate_bias, (0, HEAD_PAD - group_heads))[:, None], (HEAD_PAD, 128)
-    )
-
     kv_weights = (kv_0, kv_a, kv_b, kv_ab)
-    kv_own = project_kv(own_home, own_other, kv_weights, gate_weight, gate_bias)
+    kv_own = project_kv(own_home, own_other, kv_weights, forget_weight.T, forget_bias)
     low_own = lax.ppermute(kv_own, "sp", upward)
-    kv_par = project_kv(par_home, par_other, kv_weights, gate_weight, gate_bias)
+    kv_par = project_kv(par_home, par_other, kv_weights, forget_weight.T, forget_bias)
     low_par = lax.ppermute(kv_par, "sp", upward)
     partial = project_q((own_home, own_other, par_home, par_other), (q_0, q_a, q_b))
     blocks = (kv_own, kv_par, low_own, low_par)

time: 95.9 us -> 84 us (0.88)
  Pallas kernels: 27 us -> 12.8 us
  local copies, waits for them, and re-layouts: 7.36 us -> 2.11 us
  waiting for transfers between devices: 34.9 us -> 39.4 us
  starting transfers between devices: 25.3 us -> 29.3 us
    pallas_call x2, Pallas kernels: 13.3 us -> 7.47 us  [attend(): pl.pallas_call(functools.partial(attend_kernel, partner, scale), out_shap...]
    unnamed x28 -> x6, local copies, waits for them, and re-layouts: 3.88 us -> 0.01 us
    pallas_call x2, Pallas kernels: 6.64 us -> 3.02 us  [project_kv(): pl.pallas_call(kv_kernel, out_shape=jax.ShapeDtypeStruct((2, rows + GATE_...]
    pallas_call x1, Pallas kernels: 4.89 us -> 1.39 us  [project_q(): pl.pallas_call(q_kernel, out_shape=jax.ShapeDtypeStruct((4, rows, width),...]
    ppermute x1, starting transfers between devices: 7.13 us -> 10.3 us  [paired(): from_partner = lax.ppermute(out_par_home, 'sp', partner)]
    ppermute x1, waiting for transfers between devices: 0.01 us -> 2.43 us  [paired(): low_par = lax.ppermute(kv_par, 'sp', upward)]
    ppermute x1, waiting for transfers between devices: 0.01 us -> 1.22 us  [paired(): low_own = lax.ppermute(kv_own, 'sp', upward)]
    pallas_call x1, Pallas kernels: 2.16 us -> 0.94 us  [place(): pl.pallas_call(place_kernel, out_shape=jax.ShapeDtypeStruct((rows, 4 * wi...]
  transfers between devices with their start and end apart: 16 -> 16, of which waited for: 5 -> 7; matrix products, arithmetic and copies ran while one was open for 5% -> 3% of each run, Pallas kernels for 19% -> 10%
where the time goes in v2:
time: 84 us; the launch traced here: 83.8 us
  waiting for transfers between devices  39.4 us (47%)
  starting transfers between devices  29.3 us (35%)
  Pallas kernels  12.8 us (15%)
  local copies, waits for them, and re-layouts  2.11 us (3%)
    ppermute x1, waiting for transfers between devices, paired(): par_home = lax.ppermute(own_home, 'sp', partner)  13.3 us
    ppermute x1, starting transfers between devices, paired(): from_partner = lax.ppermute(out_par_home, 'sp', partner)  10.3 us
    ppermute x1, waiting for transfers between devices, paired(): kv_ab = lax.ppermute(kv_a, 'dp', turn)  7.93 us
    pallas_call x2, Pallas kernels, attend(): pl.pallas_call(functools.partial(attend_kernel, partner, scale), out_shap...  7.47 us
    ppermute x1, waiting for transfers between devices, paired(): from_partner = lax.ppermute(out_par_home, 'sp', partner)  5.57 us
    ppermute x1, waiting for transfers between devices, paired(): kv_a = lax.ppermute(kv_0, 'dp', hop)  5.06 us
    ppermute x1, starting transfers between devices, paired(): low_own = lax.ppermute(kv_own, 'sp', upward)  4.65 us
    ppermute x1, waiting for transfers between devices, paired(): from_across = lax.ppermute(out_par_other, ('sp', 'dp'), across)  3.82 us
  transfers between devices with their start and end apart: 16, of which 7 were waited for; matrix products, arithmetic and copies ran while one was open for 3% of the time, Pallas kernels for 10%

profile of v2, /device:TPU:0, one launch (start us, length us, event | category | flops | bytes accessed | tf_op | source)
XLA Modules:
  0.0 83.8 jit_solution(4356326494707955731)
XLA Ops:
  0.0 3.1 %collective-permute-start.1 = (bf16[192,2048]{1,0:T(8,128)(2,1)}, bf16[192,2048]{1,0:T(8,128)(2,1)S(1)}, u32[]{:S(2)}, u32[]{:S(2)}) collective-permute-start(bf16[192,2048]{1,0:T(8,128)(2,1)} %bitcast.3), channel_id=1, source_target_pairs={{0,8},{8,0},{16,24},{24,16},{1,9},{9,1},{17,25},{25,17},{2,10},{10... | collective-permute-start | bytes 2359304 | tf_op jit(solution)/shard_map/ppermute | solution.py:263
  3.1 0.0 copy-start
  3.1 0.0 copy-start.1
  3.1 0.0 copy-start.2
  3.1 1.1 %constant_dynamic-slice_fusion.5 = (bf16[256,512]{1,0:T(8,128)(2,1)S(1)}, bf16[256,512]{1,0:T(8,128)(2,1)S(1)}) fusion(bf16[256,2048]{1,0:T(8,128)(2,1)} %param.7, s32[]{:T(128)S(6)} %select_n.14, s32[]{:T(128)S(6)} %select_n.15), kind=kLoop, calls=%fused_computation.8 | loop fusion | bytes 1048584 | tf_op jit(solution)/shard_map/dynamic_slice | solution.py:255
  4.2 0.1 collective-permute-start.3
  4.3 0.5 collective-permute-start
  4.8 1.0 %constant_dynamic-slice_fusion.2 = (bf16[256,128]{1,0:T(8,128)(2,1)S(1)}, bf16[256,128]{1,0:T(8,128)(2,1)S(1)}, bf16[256,128]{1,0:T(8,128)(2,1)S(1)}, bf16[256,128]{1,0:T(8,128)(2,1)S(1)}) fusion(bf16[256,512]{1,0:T(8,128)(2,1)} %param.9, s32[]{:T(128)S(6)} %select_n.16, s32[]{:T(128)S(6)} %select_n.17, bf16[256,512]{1,0:T(8,128)(2,1)} %param.8), kind=kLoop, calls=%fused_computation.5 | loop fusion | bytes 524296 | tf_op jit(solution)/shard_map/dynamic_slice | solution.py:255
  5.8 0.1 collective-permute-start.7
  5.9 0.0 collective-permute-done.3
  6.0 1.6 %collective-permute-start.4 = (bf16[512,512]{1,0:T(8,128)(2,1)S(1)}, bf16[512,512]{1,0:T(8,128)(2,1)S(1)}, u32[]{:S(2)}, u32[]{:S(2)}) collective-permute-start(bf16[512,512]{1,0:T(8,128)(2,1)S(1)} %pad_maximum_fusion.w0_ref), channel_id=1, source_target_pairs={{0,2},{1,5},{2,0},{3,7},{4,6},{5,1},{6,4},{7,3},{8,10},{9,13},{10,... | collective-permute-start | bytes 1572872 | tf_op jit(solution)/shard_map/ppermute | solution.py:275
  7.5 13.3 %collective-permute-done.1.xc_ref.xh_ref = bf16[192,2048]{1,0:T(8,128)(2,1)S(1)} collective-permute-done((bf16[192,2048]{1,0:T(8,128)(2,1)}, bf16[192,2048]{1,0:T(8,128)(2,1)S(1)}, u32[]{:S(2)}, u32[]{:S(2)}) %collective-permute-start.1) | collective-permute-done | bytes 786464 | tf_op jit(solution)/shard_map/ppermute | solution.py:263
  20.8 0.0 collective-permute-start.2
  20.8 0.0 collective-permute-done.7
  20.8 1.7 %collective-permute-start.8 = (bf16[512,256]{1,0:T(8,128)(2,1)S(1)}, bf16[512,256]{1,0:T(8,128)(2,1)S(1)}, u32[]{:S(2)}, u32[]{:S(2)}) collective-permute-start(bf16[512,256]{1,0:T(8,128)(2,1)S(1)} %pad_maximum_fusion.1.w0_ref), channel_id=1, source_target_pairs={{0,2},{1,5},{2,0},{3,7},{4,6},{5,1},{6,4},{7,3},{8,10},{9,13},{10,... | collective-permute-start | bytes 786440 | tf_op jit(solution)/shard_map/ppermute | solution.py:265
  22.6 1.5 %collective-permute-start.9 = (bf16[512,256]{1,0:T(8,128)(2,1)S(1)}, bf16[512,256]{1,0:T(8,128)(2,1)S(1)}, u32[]{:S(2)}, u32[]{:S(2)}) collective-permute-start(bf16[512,256]{1,0:T(8,128)(2,1)S(1)} %pad_maximum_fusion.1.w0_ref), channel_id=1, source_target_pairs={{0,4},{1,3},{2,6},{3,1},{4,0},{5,7},{6,2},{7,5},{8,12},{9,11},{10,... | collective-permute-start | bytes 786440 | tf_op jit(solution)/shard_map/ppermute | solution.py:266
  24.1 5.1 %collective-permute-done.8.wa_ref = bf16[512,256]{1,0:T(8,128)(2,1)S(1)} collective-permute-done((bf16[512,256]{1,0:T(8,128)(2,1)S(1)}, bf16[512,256]{1,0:T(8,128)(2,1)S(1)}, u32[]{:S(2)}, u32[]{:S(2)}) %collective-permute-start.8) | collective-permute-done | bytes 262176 | tf_op jit(solution)/shard_map/ppermute | solution.py:265
  29.1 2.2 %collective-permute-start.5 = (bf16[512,512]{1,0:T(8,128)(2,1)S(1)}, bf16[512,512]{1,0:T(8,128)(2,1)S(1)}, u32[]{:S(2)}, u32[]{:S(2)}) collective-permute-start(bf16[512,512]{1,0:T(8,128)(2,1)S(1)} %pad_maximum_fusion.w0_ref), channel_id=1, source_target_pairs={{0,4},{1,3},{2,6},{3,1},{4,0},{5,7},{6,2},{7,5},{8,12},{9,11},{10,... | collective-permute-start | bytes 1572872 | tf_op jit(solution)/shard_map/ppermute | solution.py:276
  31.4 0.0 collective-permute-done.9.wb_ref
  31.4 0.0 collective-permute-start.10
  31.4 0.0 collective-permute-done.4.wa_ref
  31.4 2.0 %collective-permute-start.6 = (bf16[512,512]{1,0:T(8,128)(2,1)S(1)}, bf16[512,512]{1,0:T(8,128)(2,1)S(1)}, u32[]{:S(2)}, u32[]{:S(2)}) collective-permute-start(bf16[512,512]{1,0:T(8,128)(2,1)S(1)} %collective-permute-done.4.wa_ref), channel_id=1, source_target_pairs={{0,4},{1,3},{2,6},{3,1},{4,0},{5,7},{6,2},{7,5},{8,12},{9,11},{10,... | collective-permute-start | bytes 1572872 | tf_op jit(solution)/shard_map/ppermute | solution.py:277
  33.4 7.9 %collective-permute-done.10.wab_ref = bf16[512,256]{1,0:T(8,128)(2,1)S(1)} collective-permute-done((bf16[512,256]{1,0:T(8,128)(2,1)S(1)}, bf16[512,256]{1,0:T(8,128)(2,1)S(1)}, u32[]{:S(2)}, u32[]{:S(2)}) %collective-permute-start.10) | collective-permute-done | bytes 262176 | tf_op jit(solution)/shard_map/ppermute | solution.py:267
  41.4 0.0 collective-permute-done.xb_ref.xo_ref
  41.4 0.0 copy-done
  41.4 0.0 copy-done.1
  41.4 0.0 copy-done.2
  41.4 1.5 %project_kv.2.own_ref = bf16[2,208,256]{2,1,0:T(8,128)(2,1)S(1)} custom-call(bf16[192,2048]{1,0:T(8,128)(2,1)S(1)} %bitcast.5, bf16[192,2048]{1,0:T(8,128)(2,1)S(1)} %collective-permute-done.xb_ref.xo_ref, bf16[512,256]{1,0:T(8,128)(2,1)S(1)} %pad_maximum_fusion.1.w0_ref, bf16[512,256]{1,0:T(8,128)(2,1)S(1)} %collective-permute-done.8.wa_ref, ...), custom_call_target="tpu_custom_call" | custom-call | flops 402653184 | bytes 1572864 | tf_op jit(solution)/shard_map/project_kv/pallas_call | solution.py:97
  42.9 4.7 %collective-permute-start.11 = (bf16[2,208,256]{2,1,0:T(8,128)(2,1)S(1)}, bf16[2,208,256]{2,1,0:T(8,128)(2,1)S(1)}, u32[]{:S(2)}, u32[]{:S(2)}) collective-permute-start(bf16[2,208,256]{2,1,0:T(8,128)(2,1)S(1)} %project_kv.2.own_ref), channel_id=1, source_target_pairs={{0,16},{8,24},{1,17},{9,25},{2,18},{10,26},{3,19},{11,27},{4,20},{... | collective-permute-start | bytes 638984 | tf_op jit(solution)/shard_map/ppermute | solution.py:283
  47.6 0.0 collective-permute-done.2.xd_ref.xo_ref
  47.6 1.5 %project_kv.3.par_ref = bf16[2,208,256]{2,1,0:T(8,128)(2,1)S(1)} custom-call(bf16[192,2048]{1,0:T(8,128)(2,1)S(1)} %collective-permute-done.1.xc_ref.xh_ref, bf16[192,2048]{1,0:T(8,128)(2,1)S(1)} %collective-permute-done.2.xd_ref.xo_ref, bf16[512,256]{1,0:T(8,128)(2,1)S(1)} %pad_maximum_fusion.1.w0_ref, bf16[512,256]{1,0:T(8,128)(2,1)S(1)} %collective-permute-done.8.wa_ref, ...), custom_call_target="tpu_custom_call" | custom-call | flops 402653184 | bytes 1572864 | tf_op jit(solution)/shard_map/project_kv/pallas_call | solution.py:97
  49.1 1.3 %collective-permute-start.12 = (bf16[2,208,256]{2,1,0:T(8,128)(2,1)S(1)}, bf16[2,208,256]{2,1,0:T(8,128)(2,1)S(1)}, u32[]{:S(2)}, u32[]{:S(2)}) collective-permute-start(bf16[2,208,256]{2,1,0:T(8,128)(2,1)S(1)} %project_kv.3.par_ref), channel_id=1, source_target_pairs={{0,16},{8,24},{1,17},{9,25},{2,18},{10,26},{3,19},{11,27},{4,20},{... | collective-permute-start | bytes 638984 | tf_op jit(solution)/shard_map/ppermute | solution.py:285
  50.4 0.0 collective-permute-done.5.wb_ref
  50.4 1.4 %project_q.1.acc_ref = f32[4,192,512]{2,1,0:T(8,128)S(1)} custom-call(bf16[192,2048]{1,0:T(8,128)(2,1)S(1)} %bitcast.6, bf16[192,2048]{1,0:T(8,128)(2,1)S(1)} %collective-permute-done.xb_ref.xo_ref, bf16[192,2048]{1,0:T(8,128)(2,1)S(1)} %collective-permute-done.1.xc_ref.xh_ref, bf16[192,2048]{1,0:T(8,128)(2,1)S(1)} %collective-permute-done.2.xd_ref.xo_ref, ...), custom_call_target="tpu_custom_call" | custom-call | flops 1207959552 | bytes 3145728 | tf_op jit(solution)/shard_map/project_q/pallas_call | solution.py:122
  51.8 1.2 %collective-permute-done.11.lown_ref = bf16[2,208,256]{2,1,0:T(8,128)(2,1)S(1)} collective-permute-done((bf16[2,208,256]{2,1,0:T(8,128)(2,1)S(1)}, bf16[2,208,256]{2,1,0:T(8,128)(2,1)S(1)}, u32[]{:S(2)}, u32[]{:S(2)}) %collective-permute-start.11) | collective-permute-done | bytes 213024 | tf_op jit(solution)/shard_map/ppermute | solution.py:283
  53.0 0.0 collective-permute-done.6.w_ref
  53.0 2.4 %collective-permute-done.12.lpar_ref = bf16[2,208,256]{2,1,0:T(8,128)(2,1)S(1)} collective-permute-done((bf16[2,208,256]{2,1,0:T(8,128)(2,1)S(1)}, bf16[2,208,256]{2,1,0:T(8,128)(2,1)S(1)}, u32[]{:S(2)}, u32[]{:S(2)}) %collective-permute-start.12) | collective-permute-done | bytes 213024 | tf_op jit(solution)/shard_map/ppermute | solution.py:285
  55.4 3.7 %attend_own.1 = (bf16[192,512]{1,0:T(8,128)(2,1)S(1)}, bf16[192,512]{1,0:T(8,128)(2,1)S(1)}) custom-call(f32[4,192,512]{2,1,0:T(8,128)S(1)} %project_q.1.acc_ref, bf16[192,2048]{1,0:T(8,128)(2,1)S(1)} %bitcast.7, bf16[192,2048]{1,0:T(8,128)(2,1)S(1)} %collective-permute-done.xb_ref.xo_ref, bf16[512,512]{1,0:T(8,128)(2,1)S(1)} %collective-permute-done.6.w_ref, ...), custom_call_target="tpu_custom_call" | custom-call | flops 603979776 | bytes 1572864 | tf_op jit(solution)/shard_map/attend_own/pallas_call | solution.py:207
  59.2 0.1 collective-permute-start.13
  59.3 3.7 %attend_partner.1 = (bf16[192,512]{1,0:T(8,128)(2,1)S(1)}, bf16[192,512]{1,0:T(8,128)(2,1)S(1)}) custom-call(f32[4,192,512]{2,1,0:T(8,128)S(1)} %project_q.1.acc_ref, bf16[192,2048]{1,0:T(8,128)(2,1)S(1)} %collective-permute-done.1.xc_ref.xh_ref, bf16[192,2048]{1,0:T(8,128)(2,1)S(1)} %collective-permute-done.2.xd_ref.xo_ref, ...), custom_call_target="tpu_custom_call" | custom-call | flops 603979776 | bytes 1572864 | tf_op jit(solution)/shard_map/attend_partner/pallas_call | solution.py:207
  63.0 10.3 %collective-permute-start.14 = (bf16[192,512]{1,0:T(8,128)(2,1)S(1)}, bf16[192,512]{1,0:T(8,128)(2,1)S(1)}, u32[]{:S(2)}, u32[]{:S(2)}) collective-permute-start(bf16[192,512]{1,0:T(8,128)(2,1)S(1)} %get-tuple-element.11), channel_id=1, source_target_pairs={{0,8},{8,0},{16,24},{24,16},{1,9},{9,1},{17,25},{25,17},{2,10},{10... | collective-permute-start | bytes 589832 | tf_op jit(solution)/shard_map/ppermute | solution.py:291
  73.3 0.2 collective-permute-start.15
  73.4 0.0 collective-permute-done.13.b_ref
  73.4 5.6 %collective-permute-done.14.c_ref = bf16[192,512]{1,0:T(8,128)(2,1)S(1)} collective-permute-done((bf16[192,512]{1,0:T(8,128)(2,1)S(1)}, bf16[192,512]{1,0:T(8,128)(2,1)S(1)}, u32[]{:S(2)}, u32[]{:S(2)}) %collective-permute-start.14) | collective-permute-done | bytes 196640 | tf_op jit(solution)/shard_map/ppermute | solution.py:291
  79.0 3.8 %collective-permute-done.15.d_ref = bf16[192,512]{1,0:T(8,128)(2,1)S(1)} collective-permute-done((bf16[192,512]{1,0:T(8,128)(2,1)S(1)}, bf16[192,512]{1,0:T(8,128)(2,1)S(1)}, u32[]{:S(2)}, u32[]{:S(2)}) %collective-permute-start.15) | collective-permute-done | bytes 196640 | tf_op jit(solution)/shard_map/ppermute | solution.py:290
  82.8 0.9 %place.1 = bf16[192,2048]{1,0:T(8,128)(2,1)} custom-call(bf16[192,512]{1,0:T(8,128)(2,1)S(1)} %get-tuple-element.9.a_ref, bf16[192,512]{1,0:T(8,128)(2,1)S(1)} %collective-permute-done.13.b_ref, bf16[192,512]{1,0:T(8,128)(2,1)S(1)} %collective-permute-done.14.c_ref, bf16[192,512]{1,0:T(8,128)(2,1)S(1)} %collective-permute-done.15.d_ref), custom_call_target="tpu_custom_call" | custom-call | tf_op jit(solution)/shard_map/place/pallas_call | solution.py:229
  (3 shorter events, 0.1 us)
Async XLA Ops:
  0.0 20.8 %collective-permute-start.1 = (bf16[192,2048]{1,0:T(8,128)(2,1)}, bf16[192,2048]{1,0:T(8,128)(2,1)S(1)}, u32[]{:S(2)}, u32[]{:S(2)}) collective-permute-start(bf16[192,2048]{1,0:T(8,128)(2,1)} %bitcast.3), channel_id=1, source_target_pairs={{0,8},{8,0},{16,24},{24,16},{1,9},{9,1},{17,25},{25,17},{2,10},{10... | collective-permute-start | bytes 2359304 | tf_op jit(solution)/shard_map/ppermute | solution.py:263
  3.1 38.3 %copy-start = (bf16[1,192,2048]{2,1,0:T(8,128)(2,1)S(1)}, bf16[1,192,2048]{2,1,0:T(8,128)(2,1)}, u32[]{:S(2)}) copy-start(bf16[1,192,2048]{2,1,0:T(8,128)(2,1)} %param.6) | copy-start | bytes 2359300
  3.1 38.3 %copy-start.1 = (bf16[2048,16]{0,1:T(8,128)(2,1)S(1)}, bf16[2048,16]{0,1:T(8,128)(2,1)}, u32[]{:S(2)}) copy-start(bf16[2048,16]{0,1:T(8,128)(2,1)} %param.10) | copy-start | bytes 196612
  3.1 38.3 %copy-start.2 = (f32[16]{0:T(128)S(1)}, f32[16]{0:T(128)}, u32[]{:S(2)}) copy-start(f32[16]{0:T(128)} %bias_ref.3) | copy-start | bytes 196
  4.2 1.7 %collective-permute-start.3 = (bf16[256,512]{1,0:T(8,128)(2,1)S(1)}, bf16[256,512]{1,0:T(8,128)(2,1)S(1)}, u32[]{:S(2)}, u32[]{:S(2)}) collective-permute-start(bf16[256,512]{1,0:T(8,128)(2,1)S(1)} %get-tuple-element.14), channel_id=1, source_target_pairs={{0,1},{1,0},{2,3},{3,2},{4,5},{5,4},{6,7},{7,6},{8,9},{9,8},{10,11... | collective-permute-start | bytes 786440 | tf_op jit(solution)/shard_map/ppermute | solution.py:271
  4.3 37.1 %collective-permute-start = (bf16[192,2048]{1,0:T(8,128)(2,1)}, bf16[192,2048]{1,0:T(8,128)(2,1)S(1)}, u32[]{:S(2)}, u32[]{:S(2)}) collective-permute-start(bf16[192,2048]{1,0:T(8,128)(2,1)} %bitcast.4), channel_id=1, source_target_pairs={{0,1},{1,0},{2,3},{3,2},{4,5},{5,4},{6,7},{7,6},{8,9},{9,8},{10,11... | collective-permute-start | bytes 2359304 | tf_op jit(solution)/shard_map/ppermute | solution.py:278
  5.8 15.0 %collective-permute-start.7 = (bf16[256,256]{1,0:T(8,128)(2,1)S(1)}, bf16[256,256]{1,0:T(8,128)(2,1)S(1)}, u32[]{:S(2)}, u32[]{:S(2)}) collective-permute-start(bf16[256,256]{1,0:T(8,128)(2,1)S(1)} %pad_maximum_fusion.2), channel_id=1, source_target_pairs={{0,1},{1,0},{2,3},{3,2},{4,5},{5,4},{6,7},{7,6},{8,9},{9,8},{10,11... | collective-permute-start | bytes 393224 | tf_op jit(solution)/shard_map/ppermute | solution.py:264
  6.0 25.5 %collective-permute-start.4 = (bf16[512,512]{1,0:T(8,128)(2,1)S(1)}, bf16[512,512]{1,0:T(8,128)(2,1)S(1)}, u32[]{:S(2)}, u32[]{:S(2)}) collective-permute-start(bf16[512,512]{1,0:T(8,128)(2,1)S(1)} %pad_maximum_fusion.w0_ref), channel_id=1, source_target_pairs={{0,2},{1,5},{2,0},{3,7},{4,6},{5,1},{6,4},{7,3},{8,10},{9,13},{10,... | collective-permute-start | bytes 1572872 | tf_op jit(solution)/shard_map/ppermute | solution.py:275
  20.8 26.8 %collective-permute-start.2 = (bf16[192,2048]{1,0:T(8,128)(2,1)S(1)}, bf16[192,2048]{1,0:T(8,128)(2,1)S(1)}, u32[]{:S(2)}, u32[]{:S(2)}) collective-permute-start(bf16[192,2048]{1,0:T(8,128)(2,1)S(1)} %collective-permute-done.1.xc_ref.xh_ref), channel_id=1, source_target_pairs={{0,1},{1,0},{2,3},{3,2},{4,5},{5,4},{6,7},{7,6},{8,9},{9,8},{10,11... | collective-permute-start | bytes 2359304 | tf_op jit(solution)/shard_map/ppermute | solution.py:279
  20.8 8.3 %collective-permute-start.8 = (bf16[512,256]{1,0:T(8,128)(2,1)S(1)}, bf16[512,256]{1,0:T(8,128)(2,1)S(1)}, u32[]{:S(2)}, u32[]{:S(2)}) collective-permute-start(bf16[512,256]{1,0:T(8,128)(2,1)S(1)} %pad_maximum_fusion.1.w0_ref), channel_id=1, source_target_pairs={{0,2},{1,5},{2,0},{3,7},{4,6},{5,1},{6,4},{7,3},{8,10},{9,13},{10,... | collective-permute-start | bytes 786440 | tf_op jit(solution)/shard_map/ppermute | solution.py:265
  22.6 8.8 %collective-permute-start.9 = (bf16[512,256]{1,0:T(8,128)(2,1)S(1)}, bf16[512,256]{1,0:T(8,128)(2,1)S(1)}, u32[]{:S(2)}, u32[]{:S(2)}) collective-permute-start(bf16[512,256]{1,0:T(8,128)(2,1)S(1)} %pad_maximum_fusion.1.w0_ref), channel_id=1, source_target_pairs={{0,4},{1,3},{2,6},{3,1},{4,0},{5,7},{6,2},{7,5},{8,12},{9,11},{10,... | collective-permute-start | bytes 786440 | tf_op jit(solution)/shard_map/ppermute | solution.py:266
  29.1 21.2 %collective-permute-start.5 = (bf16[512,512]{1,0:T(8,128)(2,1)S(1)}, bf16[512,512]{1,0:T(8,128)(2,1)S(1)}, u32[]{:S(2)}, u32[]{:S(2)}) collective-permute-start(bf16[512,512]{1,0:T(8,128)(2,1)S(1)} %pad_maximum_fusion.w0_ref), channel_id=1, source_target_pairs={{0,4},{1,3},{2,6},{3,1},{4,0},{5,7},{6,2},{7,5},{8,12},{9,11},{10,... | collective-permute-start | bytes 1572872 | tf_op jit(solution)/shard_map/ppermute | solution.py:276
  31.4 10.0 %collective-permute-start.10 = (bf16[512,256]{1,0:T(8,128)(2,1)S(1)}, bf16[512,256]{1,0:T(8,128)(2,1)S(1)}, u32[]{:S(2)}, u32[]{:S(2)}) collective-permute-start(bf16[512,256]{1,0:T(8,128)(2,1)S(1)} %collective-permute-done.8.wa_ref), channel_id=1, source_target_pairs={{0,4},{1,3},{2,6},{3,1},{4,0},{5,7},{6,2},{7,5},{8,12},{9,11},{10,... | collective-permute-start | bytes 786440 | tf_op jit(solution)/shard_map/ppermute | solution.py:267
  31.4 21.6 %collective-permute-start.6 = (bf16[512,512]{1,0:T(8,128)(2,1)S(1)}, bf16[512,512]{1,0:T(8,128)(2,1)S(1)}, u32[]{:S(2)}, u32[]{:S(2)}) collective-permute-start(bf16[512,512]{1,0:T(8,128)(2,1)S(1)} %collective-permute-done.4.wa_ref), channel_id=1, source_target_pairs={{0,4},{1,3},{2,6},{3,1},{4,0},{5,7},{6,2},{7,5},{8,12},{9,11},{10,... | collective-permute-start | bytes 1572872 | tf_op jit(solution)/shard_map/ppermute | solution.py:277
  42.9 10.1 %collective-permute-start.11 = (bf16[2,208,256]{2,1,0:T(8,128)(2,1)S(1)}, bf16[2,208,256]{2,1,0:T(8,128)(2,1)S(1)}, u32[]{:S(2)}, u32[]{:S(2)}) collective-permute-start(bf16[2,208,256]{2,1,0:T(8,128)(2,1)S(1)} %project_kv.2.own_ref), channel_id=1, source_target_pairs={{0,16},{8,24},{1,17},{9,25},{2,18},{10,26},{3,19},{11,27},{4,20},{... | collective-permute-start | bytes 638984 | tf_op jit(solution)/shard_map/ppermute | solution.py:283
  49.1 6.4 %collective-permute-start.12 = (bf16[2,208,256]{2,1,0:T(8,128)(2,1)S(1)}, bf16[2,208,256]{2,1,0:T(8,128)(2,1)S(1)}, u32[]{:S(2)}, u32[]{:S(2)}) collective-permute-start(bf16[2,208,256]{2,1,0:T(8,128)(2,1)S(1)} %project_kv.3.par_ref), channel_id=1, source_target_pairs={{0,16},{8,24},{1,17},{9,25},{2,18},{10,26},{3,19},{11,27},{4,20},{... | collective-permute-start | bytes 638984 | tf_op jit(solution)/shard_map/ppermute | solution.py:285
  59.2 14.3 %collective-permute-start.13 = (bf16[192,512]{1,0:T(8,128)(2,1)S(1)}, bf16[192,512]{1,0:T(8,128)(2,1)S(1)}, u32[]{:S(2)}, u32[]{:S(2)}) collective-permute-start(bf16[192,512]{1,0:T(8,128)(2,1)S(1)} %get-tuple-element.10), channel_id=1, source_target_pairs={{0,1},{1,0},{2,3},{3,2},{4,5},{5,4},{6,7},{7,6},{8,9},{9,8},{10,11... | collective-permute-start | bytes 589832 | tf_op jit(solution)/shard_map/ppermute | solution.py:293
  63.0 16.0 %collective-permute-start.14 = (bf16[192,512]{1,0:T(8,128)(2,1)S(1)}, bf16[192,512]{1,0:T(8,128)(2,1)S(1)}, u32[]{:S(2)}, u32[]{:S(2)}) collective-permute-start(bf16[192,512]{1,0:T(8,128)(2,1)S(1)} %get-tuple-element.11), channel_id=1, source_target_pairs={{0,8},{8,0},{16,24},{24,16},{1,9},{9,1},{17,25},{25,17},{2,10},{10... | collective-permute-start | bytes 589832 | tf_op jit(solution)/shard_map/ppermute | solution.py:291
  73.3 9.6 %collective-permute-start.15 = (bf16[192,512]{1,0:T(8,128)(2,1)S(1)}, bf16[192,512]{1,0:T(8,128)(2,1)S(1)}, u32[]{:S(2)}, u32[]{:S(2)}) collective-permute-start(bf16[192,512]{1,0:T(8,128)(2,1)S(1)} %get-tuple-element.12), channel_id=1, source_target_pairs={{0,9},{1,8},{2,11},{3,10},{4,13},{5,12},{6,15},{7,14},{8,1},{9,0},... | collective-permute-start | bytes 589832 | tf_op jit(solution)/shard_map/ppermute | solution.py:290
